TPU v7x, 256 devices: a whole 4x4x8 slice. The times are simulated.
256 devices in a mesh: ep: 64 (over z, y, core), tp: 4 (over x).
Axes of the slice: x: 4, y: 4, z: 8, core: 2. Of those that a mesh axis runs over, the one named last changes fastest.
Arguments:
- tokens: bfloat16 [1024, 2048], P('ep'), may hold values from -6 to 6
- key_cache: bfloat16 [1024, 1024, 512], P('ep', None, 'tp'), may hold values from -6 to 6
- value_cache: bfloat16 [1024, 1024, 512], P('ep', None, 'tp'), may hold values from -6 to 6
- lengths: int32 [1024], P('ep'), may hold values from 1 to 1024, as said below
- attn_gain: float32 [2048], replicated, may hold values from 0.1 to 1.9
- query_weight: bfloat16 [2048, 1024], P('ep', 'tp'), may hold values from -0.125 to 0.125
- key_weight: bfloat16 [2048, 512], P('ep', 'tp'), may hold values from -0.125 to 0.125
- value_weight: bfloat16 [2048, 512], P('ep', 'tp'), may hold values from -0.125 to 0.125
- stay_bias: float32 [8], P('tp'), may hold values from -7.5 to -4
- out_weight: bfloat16 [1024, 2048], P('tp'), may hold values from -4 to 4
- ffn_gain: float32 [2048], replicated, may hold values from 0.1 to 1.9
- gate_weight: bfloat16 [64, 2048, 1024], P('ep', None, 'tp')
- up_weight: bfloat16 [64, 2048, 1024], P('ep', None, 'tp')
- down_weight: bfloat16 [64, 1024, 2048], P('ep', 'tp'), may hold values from -0.0234375 to 0.0234375
- routes: int32 [1024, 4], P('ep'), may hold values from 0 to 63, as said below
- route_weight: float32 [1024, 4], P('ep'), may hold values from 0.05 to 1
Outputs:
- layer_out: bfloat16 [1024, 2048], P('ep', 'tp')
- new_keys: bfloat16 [1024, 512], P('ep', 'tp')
- new_values: bfloat16 [1024, 512], P('ep', 'tp')
Inputs may be any that keep to these rules, and one draw needn't show every extreme that they name: `lengths`: the sequences of every index of ep include one with length 1024. `routes`: each row names 4 different experts; the rows of one device (aligned blocks of 16 rows) name any one expert at most 2 times; in every draw one expert is named exactly 2 times by the rows of every device.
All inputs are finite; a program needn't handle non-finite values.
Results may differ from a plain program's by a relative error of at most 0.018.
Values may be sent and summed in bfloat16 or wider, within the bound.
A program may use at most 64 MiB of HBM per device.

v0:
```python
import jax
import jax.numpy as jnp
from jax import lax
from jax.sharding import Mesh
from jax.sharding import PartitionSpec as P

HQ = 8
KVH = 4
HD = 128
TOPK = 4
EP = ("ep_0", "ep_1", "ep_2")


eps_norm = 1e-05
clamp_limit = 7.0
gate_alpha = 1.702


def copy_for_each(array, axis):
    copies = jnp.broadcast_to(array, (lax.axis_size(axis), *array.shape))
    return lax.all_to_all(copies, axis, split_axis=0, concat_axis=0, tiled=True)


def joined_along(pieces, dim):
    pieces = jnp.moveaxis(pieces, 0, dim)
    dims = pieces.shape
    return pieces.reshape(*dims[:dim], dims[dim] * dims[dim + 1], *dims[dim + 2 :])


def gathered_by_axis(array, axes, dim):
    far, near = axes
    pieces = copy_for_each(copy_for_each(array, far), near)
    return joined_along(pieces.swapaxes(0, 1).reshape(-1, *array.shape), dim)


def in_one_piece(arrays, axis, dim, along):
    widths = [a.shape[along] for a in arrays]
    both = jnp.concatenate(arrays, axis=along)
    whole = gathered_by_axis(both, axis, dim)
    return tuple(jnp.split(whole, [sum(widths[:k]) for k in range(1, len(widths))], axis=along))


def taken_together(array, axis):
    everything = copy_for_each(array, axis)
    return jnp.sum(everything.astype(jnp.float32), axis=0)


def split_up(array, dim, devices):
    dims = array.shape
    pieces = array.reshape(*dims[:dim], devices, dims[dim] // devices, *dims[dim + 1 :])
    return jnp.moveaxis(pieces, dim, 0)


def sent_and_summed(array, axis, dim):
    pieces = split_up(array, dim, lax.axis_size(axis))
    arrived = lax.all_to_all(pieces, axis, split_axis=0, concat_axis=0, tiled=True)
    return arrived.astype(jnp.float32).sum(axis=0)


def rms_scale(values, gain):
    floats = values.astype(jnp.float32)
    scaled = floats * lax.rsqrt(jnp.mean(floats * floats, axis=-1, keepdims=True) + eps_norm)
    return scaled * gain


def stick_weights(scores, live_mask):
    log_stay = jnp.where(live_mask, jax.nn.log_sigmoid(-scores), 0.0)
    later_sum = lax.cumsum(log_stay, axis=scores.ndim - 1, reverse=True) - log_stay
    return jnp.where(live_mask, jnp.exp(jax.nn.log_sigmoid(scores) + later_sum), 0.0)


def expert_units(gate_pre, upward):
    capped = jnp.minimum(gate_pre, clamp_limit)
    upward = jnp.clip(upward, -clamp_limit, clamp_limit)
    return capped * jax.nn.sigmoid(gate_alpha * capped) * (upward + 1.0)


def body(
    tokens,
    key_cache,
    value_cache,
    lengths,
    attn_gain,
    query_weight,
    key_weight,
    value_weight,
    stay_bias,
    out_weight,
    ffn_gain,
    gate_weight,
    up_weight,
    down_weight,
    routes,
    route_weight,
):
    seq_count, model_width = tokens.shape
    tp_size = lax.axis_size("tp")
    heads_here = HQ // tp_size
    kv_here = KVH // tp_size
    group_size = HQ // KVH
    query_cols = heads_here * HD
    normed = rms_scale(tokens, attn_gain).astype(jnp.bfloat16)
    whole_query, whole_key, whole_value = in_one_piece(
        (query_weight, key_weight, value_weight), (("ep_0", "ep_1"), "ep_2"), 0, 1
    )
    queries = jnp.dot(normed, whole_query, preferred_element_type=jnp.float32).astype(jnp.bfloat16)
    new_keys = jnp.dot(normed, whole_key, preferred_element_type=jnp.float32).astype(jnp.bfloat16)
    new_values = jnp.dot(normed, whole_value, preferred_element_type=jnp.float32).astype(
        jnp.bfloat16
    )
    cache_len = key_cache.shape[1]
    grouped = queries.reshape(seq_count, kv_here, group_size, HD)
    key_rows = key_cache.reshape(seq_count, cache_len, kv_here, HD)
    value_rows = value_cache.reshape(seq_count, cache_len, kv_here, HD)
    scores = jnp.einsum(
        "skgd,sckd->skgc", grouped, key_rows, preferred_element_type=jnp.float32
    ) * HD ** (-0.5)
    scores = scores + stay_bias.reshape(kv_here, group_size)[None, :, :, None]
    positions = jnp.arange(cache_len, dtype=jnp.int32)
    live_mask = positions[None, None, None, :] < lengths[:, None, None, None]
    weights = stick_weights(scores, live_mask).astype(jnp.bfloat16)
    attended = jnp.einsum(
        "skgc,sckd->skgd", weights, value_rows, preferred_element_type=jnp.float32
    )
    attended = attended.astype(jnp.bfloat16).reshape(seq_count, query_cols)
    head_mix = taken_together(
        jnp.dot(attended, out_weight, preferred_element_type=jnp.float32).astype(jnp.bfloat16), "tp"
    ).astype(jnp.float32)
    residual = (tokens.astype(jnp.float32) + head_mix).astype(jnp.bfloat16)
    ffn_in = rms_scale(residual, ffn_gain).astype(jnp.bfloat16)
    slice_width = model_width // tp_size
    local_experts = gate_weight.shape[0]
    experts_all = local_experts * lax.axis_size(EP)
    capacity = min(seq_count, 2 * max(1, seq_count * TOPK // experts_all))
    expert_ids = jnp.arange(experts_all, dtype=jnp.int32)
    flat_routes = routes.reshape(-1)
    matches = (flat_routes[:, None] == expert_ids[None, :]).astype(jnp.int32)
    before = jnp.cumsum(matches, axis=0) - matches
    slot_rank = jnp.sum(before * matches, axis=1)
    slot_index = flat_routes * capacity + slot_rank
    slot_ids = jnp.arange(experts_all * capacity, dtype=jnp.int32)
    placing = jnp.any(
        slot_index.reshape(seq_count, TOPK)[:, :, None] == slot_ids[None, None, :], axis=1
    )
    outgoing = jnp.einsum(
        "ts,td->sd", placing.astype(jnp.bfloat16), ffn_in, preferred_element_type=jnp.float32
    )
    outgoing = outgoing.astype(jnp.bfloat16).reshape(experts_all, capacity, ffn_in.shape[1])
    received = lax.all_to_all(outgoing, EP, split_axis=0, concat_axis=0, tiled=True)
    item_count = received.shape[1]
    stacked = received.reshape(-1, local_experts, item_count, model_width)
    gate_pre = jnp.einsum(
        "nxcd,xdf->nxcf", stacked, gate_weight, preferred_element_type=jnp.float32
    )
    upward = jnp.einsum("nxcd,xdf->nxcf", stacked, up_weight, preferred_element_type=jnp.float32)
    unit_out = expert_units(gate_pre, upward).astype(jnp.bfloat16)
    partial_out = jnp.einsum(
        "nxcf,xfd->nxcd", unit_out, down_weight, preferred_element_type=jnp.float32
    )
    partial_out = partial_out.reshape(-1, item_count, model_width)
    summed = sent_and_summed(partial_out.astype(jnp.bfloat16), "tp", 2).astype(jnp.bfloat16)
    returned = lax.all_to_all(summed, EP, split_axis=0, concat_axis=0, tiled=True)
    picked_rows = returned.reshape(experts_all * capacity, slice_width)[slot_index]
    picked_rows = picked_rows.astype(jnp.float32).reshape(seq_count, TOPK, slice_width)
    routed_sum = jnp.sum(picked_rows * route_weight[:, :, None], axis=1)
    own_slice = lax.dynamic_slice_in_dim(
        residual, lax.axis_index("tp") * slice_width, slice_width, 1
    )
    layer_out = (own_slice.astype(jnp.float32) + routed_sum).astype(jnp.bfloat16)
    return (layer_out, new_keys, new_values)


def solution(mesh):
    finer = Mesh(mesh.devices.reshape(8, 4, 2, mesh.shape["tp"]), ("ep_0", "ep_1", "ep_2", "tp"))
    placed = (
        P(EP, None),
        P(EP, None, "tp"),
        P(EP, None, "tp"),
        P(EP),
        P(),
        P(EP, "tp"),
        P(EP, "tp"),
        P(EP, "tp"),
        P("tp"),
        P("tp", None),
        P(),
        P(EP, None, "tp"),
        P(EP, None, "tp"),
        P(EP, "tp", None),
        P(EP, None),
        P(EP, None),
    )
    return jax.shard_map(
        body,
        mesh=finer,
        in_specs=placed,
        out_specs=(P(EP, "tp"), P(EP, "tp"), P(EP, "tp")),
        check_vma=False,
    )
```

profile of v0, /device:TPU:1, one launch (start us, length us, event | category | flops | bytes accessed | tf_op | source)
XLA Modules:
  0.0 174.6 jit_solution(14970936008968026358)
XLA Ops:
  0.7 0.8 pad_maximum_fusion
  1.5 1.1 broadcast_in_dim.34
  2.6 12.0 %all-to-all-start = ((bf16[32,32,512]{2,1,0:T(8,128)(2,1)}), bf16[32,32,512]{2,1,0:T(8,128)(2,1)S(1)}, u32[]{:S(2)}, u32[]{:S(2)}) async-start(bf16[32,32,512]{2,1,0:T(8,128)(2,1)} %broadcast_in_dim.34), calls=%async_computation | async-start | bytes 2097152 | tf_op jit(solution)/shard_map/all_to_all | solution.py:21
  15.5 25.3 %all-to-all-done = bf16[32,32,512]{2,1,0:T(8,128)(2,1)S(1)} async-done(((bf16[32,32,512]{2,1,0:T(8,128)(2,1)}), bf16[32,32,512]{2,1,0:T(8,128)(2,1)S(1)}, u32[]{:S(2)}, u32[]{:S(2)}) %all-to-all-start) | async-done | bytes 1048608 | tf_op jit(solution)/shard_map/all_to_all | solution.py:21
  41.1 7.9 %all_to_all.30 = bf16[2,32,32,512]{3,2,1,0:T(8,128)(2,1)S(1)} all-to-all(bf16[2,32,32,512]{3,2,1,0:T(8,128)(2,1)S(1)} %broadcast_in_dim.35), channel_id=1, replica_groups=mesh['ep_0'=8,'ep_1'=4,'ep_2'=2,'tp'=4] {'ep_2'}, dimensions={0} | all-to-all | bytes 4194304 | tf_op jit(solution)/shard_map/all_to_all | solution.py:21
  49.2 1.3 copy-done.1
  50.9 3.4 %fusion.30 = (f32[16,2,1024]{2,1,0:T(2,128)S(1)}, f32[16,2,1024]{2,1,0:T(2,128)S(1)}) fusion(pred[16,1024]{1,0:T(8,128)(4,1)S(1)} %iota_compare_fusion, f32[2]{0:T(128)S(1)} %copy-done.9, bf16[16,2,128]{2,1,0:T(2,128)(2,1)S(1)} %reshape.196, bf16[16,1024,128]{2,1,0:T(8,128)(2,1)} %param.17), kind=kOutput, calls=%fused_computation.47 | convolution fusion | flops 8716288 | bytes 4481032 | tf_op jit(solution)/shard_map/skgd,sckd->skgc/dot_general | solution.py:115
  54.4 39.6 %reduce-window.6 = f32[16,1,2,8,128]{4,3,2,1,0:T(8,128)S(1)} reduce-window(f32[16,1,2,8,128]{4,3,2,1,0:T(8,128)S(1)} %bitcast.83, f32[]{:T(128)} %constant.16.clone.1), window={size=1x1x1x1x128 pad=0_0x0_0x0_0x0_0x0_127}, to_apply=%region_1.2 | reduce-window | flops 4161536 | bytes 262148 | tf_op jit(solution)/shard_map/reduce-window
  94.6 3.3 %convolution_convert_fusion.3 = bf16[16,2,128]{2,1,0:T(2,128)(2,1)S(1)} fusion(bf16[16,1024,128]{2,1,0:T(8,128)(2,1)} %param.18, pred[16,1024]{1,0:T(8,128)(4,1)S(1)} %iota_compare_fusion, f32[16,2,1024]{2,1,0:T(2,128)S(1)} %reshape.198, f32[16,2,1024]{2,1,0:T(2,128)S(1)} %reshape.201, f32[16,2,1024]{2,1,0:T(2,128)S(1)} %get-tuple-element.8), kind=kOutput, calls=%fused_computation.15 | convolution fusion | flops 9080832 | bytes 4612096 | tf_op jit(solution)/shard_map/skgc,sckd->skgd/dot_general | solution.py:122
  98.9 4.0 %all-to-all-start.2 = ((bf16[4,16,2048]{2,1,0:T(8,128)(2,1)}), bf16[4,16,2048]{2,1,0:T(8,128)(2,1)S(1)}, u32[]{:S(2)}, u32[]{:S(2)}) async-start(bf16[4,16,2048]{2,1,0:T(8,128)(2,1)} %broadcast_in_dim.36), calls=%async_computation.2 | async-start | bytes 524288 | tf_op jit(solution)/shard_map/all_to_all | solution.py:21
  103.1 5.6 %all-to-all-done.2 = bf16[4,16,2048]{2,1,0:T(8,128)(2,1)S(1)} async-done(((bf16[4,16,2048]{2,1,0:T(8,128)(2,1)}), bf16[4,16,2048]{2,1,0:T(8,128)(2,1)S(1)}, u32[]{:S(2)}, u32[]{:S(2)}) %all-to-all-start.2) | async-done | bytes 262176 | tf_op jit(solution)/shard_map/all_to_all | solution.py:21
  109.7 25.0 %all_to_all.31 = bf16[64,2,2048]{2,1,0:T(2,128)(2,1)S(1)} all-to-all(bf16[64,2,2048]{2,1,0:T(2,128)(2,1)S(1)} %reshape.203), channel_id=1, replica_groups=mesh['ep_0'=8,'ep_1'=4,'ep_2'=2,'tp'=4] {'ep_0','ep_1','ep_2'}, dimensions={0} | all-to-all | bytes 1048576 | tf_op jit(solution)/shard_map/all_to_all | solution.py:149
  134.7 1.6 fusion.4
  136.3 0.8 fusion
  137.1 1.2 convert_element_type.98
  138.3 2.1 %copy.80 = bf16[64,2,4,512]{3,0,1,2:T(8,128)(2,1)} copy(bf16[64,2,4,512]{3,2,0,1:T(4,128)(2,1)} %convert_element_type.98) | data formatting | bytes 1048576 | tf_op jit(solution)/shard_map/convert_element_type | solution.py:161
  140.4 4.1 %all-to-all-start.4 = ((bf16[4,64,2,512]{3,1,2,0:T(8,128)(2,1)}), bf16[4,64,2,512]{3,1,2,0:T(8,128)(2,1)}, u32[]{:S(2)}, u32[]{:S(2)}) async-start(bf16[4,64,2,512]{3,1,2,0:T(8,128)(2,1)} %bitcast.81), calls=%async_computation.4 | async-start | bytes 1048576 | tf_op jit(solution)/shard_map/all_to_all | solution.py:56
  144.7 9.0 %all-to-all-done.4 = bf16[4,64,2,512]{3,1,2,0:T(8,128)(2,1)} async-done(((bf16[4,64,2,512]{3,1,2,0:T(8,128)(2,1)}), bf16[4,64,2,512]{3,1,2,0:T(8,128)(2,1)}, u32[]{:S(2)}, u32[]{:S(2)}) %all-to-all-start.4) | async-done | bytes 524320 | tf_op jit(solution)/shard_map/all_to_all | solution.py:56
  153.8 1.1 reduce_sum.66
  154.9 0.8 copy.66
  155.7 6.2 %all-to-all-start.5 = ((bf16[64,2,512]{2,1,0:T(2,128)(2,1)}), bf16[64,2,512]{2,1,0:T(2,128)(2,1)S(1)}, u32[]{:S(2)}, u32[]{:S(2)}) async-start(bf16[64,2,512]{2,1,0:T(2,128)(2,1)} %copy.66), calls=%async_computation.5 | async-start | bytes 262144 | tf_op jit(solution)/shard_map/all_to_all | solution.py:162
  161.9 0.8 convolution_convert_fusion.5
  162.7 0.8 convolution_convert_fusion.6
  163.6 9.4 %all-to-all-done.5 = bf16[64,2,512]{2,1,0:T(2,128)(2,1)S(1)} async-done(((bf16[64,2,512]{2,1,0:T(2,128)(2,1)}), bf16[64,2,512]{2,1,0:T(2,128)(2,1)S(1)}, u32[]{:S(2)}, u32[]{:S(2)}) %all-to-all-start.5) | async-done | bytes 131104 | tf_op jit(solution)/shard_map/all_to_all | solution.py:162
  (63 shorter events, 6.1 us)
Async XLA Ops:
  0.6 135.7 %copy-start = (bf16[1,256,2048]{2,1,0:T(8,128)(2,1)S(1)}, bf16[1,256,2048]{2,1,0:T(8,128)(2,1)}, u32[]{:S(2)}) copy-start(bf16[1,256,2048]{2,1,0:T(8,128)(2,1)} %param.29) | copy-start | bytes 3145732
  0.6 14.0 %copy-start.7 = (s32[16,4]{0,1:T(4,128)S(1)}, s32[16,4]{0,1:T(4,128)}, u32[]{:S(2)}) copy-start(s32[16,4]{0,1:T(4,128)} %param.30) | copy-start | bytes 772
  0.7 14.6 %copy-start.5 = (bf16[16,2048]{1,0:T(8,128)(2,1)S(1)}, bf16[16,2048]{1,0:T(8,128)(2,1)}, u32[]{:S(2)}) copy-start(bf16[16,2048]{1,0:T(8,128)(2,1)} %param.16) | copy-start | bytes 196612
  0.7 14.8 %copy-start.10 = (s32[16]{0:T(128)S(1)}, s32[16]{0:T(128)}, u32[]{:S(2)}) copy-start(s32[16]{0:T(128)} %param.19) | copy-start | bytes 196
  2.6 38.2 %all-to-all-start = ((bf16[32,32,512]{2,1,0:T(8,128)(2,1)}), bf16[32,32,512]{2,1,0:T(8,128)(2,1)S(1)}, u32[]{:S(2)}, u32[]{:S(2)}) async-start(bf16[32,32,512]{2,1,0:T(8,128)(2,1)} %broadcast_in_dim.34), calls=%async_computation | async-start | bytes 2097152 | tf_op jit(solution)/shard_map/all_to_all | solution.py:21
  49.0 1.6 copy-start.11
  49.0 1.9 %copy-start.9 = (f32[2]{0:T(128)S(1)}, f32[2]{0:T(128)}, u32[]{:S(2)}) copy-start(f32[2]{0:T(128)} %param.24) | copy-start | bytes 28
  49.2 1.4 copy-start.1
  94.6 3.3 %copy-start.4 = (bf16[256,2048]{1,0:T(8,128)(2,1)S(1)}, bf16[256,2048]{1,0:T(8,128)(2,1)}, u32[]{:S(2)}) copy-start(bf16[256,2048]{1,0:T(8,128)(2,1)} %param.25) | copy-start | bytes 3145732
  97.9 11.0 %copy-start.6 = (f32[2048]{0:T(1024)S(1)}, f32[2048]{0:T(1024)}, u32[]{:S(2)}) copy-start(f32[2048]{0:T(1024)} %param.26) | copy-start | bytes 24580
  98.9 9.8 %all-to-all-start.2 = ((bf16[4,16,2048]{2,1,0:T(8,128)(2,1)}), bf16[4,16,2048]{2,1,0:T(8,128)(2,1)S(1)}, u32[]{:S(2)}, u32[]{:S(2)}) async-start(bf16[4,16,2048]{2,1,0:T(8,128)(2,1)} %broadcast_in_dim.36), calls=%async_computation.2 | async-start | bytes 524288 | tf_op jit(solution)/shard_map/all_to_all | solution.py:21
  109.0 27.4 %copy-start.3 = (bf16[1,2048,256]{2,1,0:T(8,128)(2,1)S(1)}, bf16[1,2048,256]{2,1,0:T(8,128)(2,1)}, u32[]{:S(2)}) copy-start(bf16[1,2048,256]{2,1,0:T(8,128)(2,1)} %param.28) | copy-start | bytes 3145732
  137.1 7.5 %copy-start.8 = (f32[16,4]{0,1:T(4,128)S(1)}, f32[16,4]{0,1:T(4,128)}, u32[]{:S(2)}) copy-start(f32[16,4]{0,1:T(4,128)} %param.31) | copy-start | bytes 772
  138.3 23.6 %copy-start.2 = (bf16[2,32,32,512]{3,2,0,1:T(8,128)(2,1)S(1)}, bf16[2,32,32,512]{3,2,0,1:T(8,128)(2,1)}, u32[]{:S(2)}) copy-start(bf16[2,32,32,512]{3,2,0,1:T(8,128)(2,1)} %copy-done.1) | copy-start | bytes 6291460
  140.4 13.4 %all-to-all-start.4 = ((bf16[4,64,2,512]{3,1,2,0:T(8,128)(2,1)}), bf16[4,64,2,512]{3,1,2,0:T(8,128)(2,1)}, u32[]{:S(2)}, u32[]{:S(2)}) async-start(bf16[4,64,2,512]{3,1,2,0:T(8,128)(2,1)} %bitcast.81), calls=%async_computation.4 | async-start | bytes 1048576 | tf_op jit(solution)/shard_map/all_to_all | solution.py:56
  155.7 17.3 %all-to-all-start.5 = ((bf16[64,2,512]{2,1,0:T(2,128)(2,1)}), bf16[64,2,512]{2,1,0:T(2,128)(2,1)S(1)}, u32[]{:S(2)}, u32[]{:S(2)}) async-start(bf16[64,2,512]{2,1,0:T(2,128)(2,1)} %copy.66), calls=%async_computation.5 | async-start | bytes 262144 | tf_op jit(solution)/shard_map/all_to_all | solution.py:162
where the time goes:
time: 175 us
  waiting for transfers between devices  49.4 us (28%)
  other arithmetic  43.2 us (25%)
  blocking collectives  32.9 us (19%)
  starting transfers between devices  26.3 us (15%)
  matrix products  11.6 us (7%)
  local copies, waits for them, and re-layouts  10.1 us (6%)
    another operation x2, other arithmetic  39.7 us
    all_to_all x2, waiting for transfers between devices, copy_for_each(): return lax.all_to_all(copies, axis, split_axis=0, concat_axis=0, tiled=True)  31 us
    all_to_all x1, blocking collectives, body(): lax.all_to_all(outgoing, EP, split_axis=0, concat_axis=0, tiled=True)  25 us
    all_to_all x2, starting transfers between devices, copy_for_each(): return lax.all_to_all(copies, axis, split_axis=0, concat_axis=0, tiled=True)  16 us
    all_to_all x1, waiting for transfers between devices, body(): lax.all_to_all(summed, EP, split_axis=0, concat_axis=0, tiled=True)  9.41 us
    all_to_all x1, waiting for transfers between devices, sent_and_summed(): lax.all_to_all(pieces, axis, split_axis=0, concat_axis=0, tiled=True)  9.04 us
    all_to_all x1, blocking collectives, copy_for_each(): return lax.all_to_all(copies, axis, split_axis=0, concat_axis=0, tiled=True)  7.85 us
    all_to_all x1, starting transfers between devices, body(): lax.all_to_all(summed, EP, split_axis=0, concat_axis=0, tiled=True)  6.19 us
  transfers between devices with their start and end apart: 4, of which 4 were waited for; matrix products, arithmetic and copies ran while one was open for 2% of the time, Pallas kernels for 0%

commit v1 on v0

v1 whole, which is shorter than its diff:
```python
import functools
import math

import jax
import jax.numpy as jnp
from jax import lax
from jax.experimental import pallas as pl
from jax.experimental.pallas import tpu as pltpu
from jax.sharding import Mesh
from jax.sharding import PartitionSpec as P

AXES = ("ep_0", "ep_1", "ep_2", "tp")
EP = AXES[:3]
MESH = pl.DeviceIdType.MESH
F32 = jnp.float32
BF16 = jnp.bfloat16
HD = 128
CAP = 2
eps_norm = 1e-05
clamp_limit = 7.0
gate_alpha = 1.702


def dot(a, b, dims=((1,), (0,))):
    return lax.dot_general(a, b, (dims, ((), ())), preferred_element_type=F32)


def rms_scale(values, gain):
    scale = lax.rsqrt(jnp.mean(values * values, axis=-1, keepdims=True) + eps_norm)
    return values * scale * gain


def iota(shape, dim):
    return lax.broadcasted_iota(jnp.int32, shape, dim)


def layer_kernel(
    sizes,
    tokens, key_cache, value_cache, lengths, attn_gain, query_weight, key_weight, value_weight,
    stay_bias, out_weight, ffn_gain, gate_weight, up_weight, down_weight, routes, route_weight,
    layer_out, new_keys, new_values,
    tok, gain_a, gain_f, route_v, rweight_v, kc, vc, ow, gw, uw, dw,
    normed, slices, wq, wkv, part_q, part_kv, got_q, got_kv,
    sticks, hp, hr, sb, xg, epart, egot, rb, rt,
    loc, kv_sem, exp_sem, send, recv, chunk_recv, group_recv, group_got,
):
    NZ, NY, NC, NX = sizes
    NP = NY * NC
    NE = NZ * NP
    z, y, c, x = (lax.axis_index(a) for a in AXES)
    yc = y * NC + c
    me = z * NP + yc
    seqs, width = tok.shape
    kblock = width // NZ
    quarter = width // NX
    QB = quarter // HD
    cache_len = kc.shape[1]
    RB = CAP * QB
    topk = route_v.shape[1]

    def zplus(d):
        return lax.rem(z + d, NZ)

    def pplus(i):
        j = lax.rem(yc + i, NP)
        return j, {"ep_1": j // NC, "ep_2": lax.rem(j, NC)}

    def xplus(d):
        return lax.rem(x + d, NX)

    barrier = pltpu.get_barrier_semaphore()
    for d in range(1, NZ):
        pl.semaphore_signal(barrier, inc=1, device_id={"ep_0": zplus(d)}, device_id_type=MESH)
    for i in range(1, NP):
        pl.semaphore_signal(barrier, inc=1, device_id=pplus(i)[1], device_id_type=MESH)
    for d in range(1, NX):
        pl.semaphore_signal(barrier, inc=1, device_id={"tp": xplus(d)}, device_id_type=MESH)

    def load(src, dst, sem):
        copy = pltpu.make_async_copy(src, dst, sem)
        copy.start()
        return copy

    ld_tok = load(tokens, tok, loc.at[0])
    ld_ga = load(attn_gain, gain_a, loc.at[1])
    ld_wq = load(query_weight, wq.at[yc], loc.at[2])
    ld_wk = load(key_weight, wkv.at[yc, :, pl.ds(0, HD)], loc.at[3])
    ld_wv = load(value_weight, wkv.at[yc, :, pl.ds(HD, HD)], loc.at[4])
    ld_rt = load(routes, route_v, loc.at[5])
    ld_rw = load(route_weight, rweight_v, loc.at[6])
    ld_gf = load(ffn_gain, gain_f, loc.at[7])
    npair = seqs // 2
    ld_k = [load(key_cache.at[pl.ds(2 * p, 2)], kc.at[pl.ds(2 * p, 2)], kv_sem.at[0, p]) for p in range(npair)]
    ld_v = [load(value_cache.at[pl.ds(2 * p, 2)], vc.at[pl.ds(2 * p, 2)], kv_sem.at[1, p]) for p in range(npair)]
    ld_ow = load(out_weight, ow, exp_sem.at[0])
    ld_gw = load(gate_weight.at[0], gw, exp_sem.at[1])
    ld_uw = load(up_weight.at[0], uw, exp_sem.at[2])
    ld_dw = load(down_weight.at[0], dw, exp_sem.at[3])

    def remote(src, dst, s, r, device):
        return pltpu.make_async_remote_copy(
            src_ref=src, dst_ref=dst, send_sem=s, recv_sem=r, device_id=device, device_id_type=MESH
        )

    def wait_bytes(ref, sem):
        pltpu.make_async_copy(ref, ref, sem).wait()

    ld_tok.wait()
    ld_ga.wait()
    normed[...] = rms_scale(tok[...].astype(F32), gain_a[...]).astype(BF16)
    ld_wq.wait()
    pl.semaphore_wait(barrier, NZ - 1 + NP - 1 + NX - 1)
    far = sorted(range(1, NZ), key=lambda d: -min(d, NZ - d))
    for d in far:
        zt = zplus(d)
        remote(
            normed.at[:, pl.ds(pl.multiple_of(zt * kblock, kblock), kblock)], slices.at[z],
            send.at[0], recv.at[0], {"ep_0": zt},
        ).start()
    for i in range(1, NP):
        remote(wq.at[yc], wq.at[yc], send.at[1], recv.at[1], pplus(i)[1]).start()
    ld_wk.wait()
    ld_wv.wait()
    for i in range(1, NP):
        remote(wkv.at[yc], wkv.at[yc], send.at[2], recv.at[2], pplus(i)[1]).start()
    slices[pl.ds(z, 1)] = normed[:, pl.ds(pl.multiple_of(z * kblock, kblock), kblock)][None]

    wait_bytes(slices.at[pl.ds(0, NZ - 1)], recv.at[0])
    wait_bytes(wq.at[pl.ds(0, NP - 1)], recv.at[1])
    lhs = slices[...].reshape(NZ * seqs, kblock)
    part_q[...] = dot(lhs, wq[...].reshape(kblock, 2 * HD)).astype(BF16).reshape(NZ, seqs, 2 * HD)
    for d in far:
        zt = zplus(d)
        remote(part_q.at[zt], got_q.at[z], send.at[3], recv.at[3], {"ep_0": zt}).start()
    got_q[pl.ds(z, 1)] = part_q[pl.ds(z, 1)]

    wait_bytes(wkv.at[pl.ds(0, NP - 1)], recv.at[2])
    part_kv[...] = dot(lhs, wkv[...].reshape(kblock, 2 * HD)).astype(BF16).reshape(NZ, seqs, 2 * HD)
    for d in far:
        zt = zplus(d)
        remote(part_kv.at[zt], got_kv.at[z], send.at[4], recv.at[4], {"ep_0": zt}).start()
    got_kv[pl.ds(z, 1)] = part_kv[pl.ds(z, 1)]

    rows, cols = QB * seqs, NE * RB
    ld_rt.wait()
    ld_rw.wait()
    route = jnp.concatenate([route_v[...]] * QB, axis=0)
    rweight = jnp.concatenate([rweight_v[...]] * QB, axis=0)
    col = iota((rows, cols), 1)
    row = iota((rows, cols), 0)
    col_e = col // RB
    hit = jnp.zeros((rows, cols), F32)
    weighted = jnp.zeros((rows, cols), F32)
    for k in range(topk):
        same = route[:, k : k + 1] == col_e
        hit = jnp.where(same, 1.0, hit)
        weighted = jnp.where(same, rweight[:, k : k + 1], weighted)
    r0, r1 = iota((rows, rows), 0), iota((rows, rows), 1)
    earlier = ((r0 // seqs == r1 // seqs) & (r1 < r0)).astype(F32).astype(BF16)
    before = dot(earlier, hit.astype(BF16))
    chosen = (row // seqs == lax.rem(col, QB)) & (
        before == (lax.rem(col, RB) // QB).astype(F32)
    )
    place = jnp.where(chosen, hit, 0.0).astype(BF16)
    weighted = jnp.where(chosen, weighted, 0.0)
    weight_hi = weighted.astype(BF16)
    weight_lo = (weighted - weight_hi.astype(F32)).astype(BF16)

    hrow = iota((2 * seqs, 1), 0)
    seq_of = lax.rem(hrow, seqs)
    length_col = jnp.zeros((2 * seqs, 1), jnp.int32)
    for s in range(seqs):
        length_col = jnp.where(seq_of == s, lengths[s], length_col)
    bias_col = jnp.where(hrow < seqs, stay_bias[0], stay_bias[1])

    wait_bytes(got_q.at[pl.ds(0, NZ - 1)], recv.at[3])
    query = jnp.sum(got_q[...].astype(F32), axis=0)
    query = jnp.concatenate([query[:, :HD], query[:, HD:]], axis=0).astype(BF16).astype(F32)
    twice = jnp.concatenate([query, query], axis=1)
    pair_row = lax.rem(iota((2 * seqs, 2 * HD), 0), seqs) - iota((2 * seqs, 2 * HD), 1) // HD
    total = None
    for p in range(npair):
        ld_k[p].wait()
        block = jnp.where(pair_row == 2 * p, twice, 0.0).astype(BF16)
        keys = jnp.concatenate([kc[2 * p], kc[2 * p + 1]], axis=1)
        term = dot(block, keys, ((1,), (1,)))
        total = term if total is None else total + term
    zs = total * (HD ** -0.5) + bias_col
    live = iota((2 * seqs, cache_len), 1) < length_col
    log_stay = jnp.where(live, -(jnp.maximum(zs, 0.0) + jnp.log1p(jnp.exp(-jnp.abs(zs)))), 0.0)
    hi = log_stay.astype(BF16)
    lo = (log_stay - hi.astype(F32)).astype(BF16)
    blk = min(256, cache_len)
    tri = (iota((blk, blk), 0) >= iota((blk, blk), 1)).astype(F32).astype(BF16)
    carry = jnp.zeros((2 * seqs, 1), F32)
    for b in reversed(range(cache_len // blk)):
        at = slice(b * blk, (b + 1) * blk)
        within = dot(hi[:, at], tri) + dot(lo[:, at], tri)
        stick = jnp.where(live[:, at], jnp.exp(zs[:, at] + within + carry), 0.0)
        sticks[:, at] = stick.astype(BF16)
        carry = carry + within[:, 0:1]
    weights = sticks[...]
    att = jnp.zeros((2 * seqs, HD), F32)
    for p in range(npair):
        ld_v[p].wait()
        values = jnp.concatenate([vc[2 * p], vc[2 * p + 1]], axis=1)
        mixed = dot(weights, values)
        att = att + jnp.where(seq_of == 2 * p, mixed[:, :HD], 0.0)
        att = att + jnp.where(seq_of == 2 * p + 1, mixed[:, HD:], 0.0)
    att = att.astype(BF16)
    attended = jnp.concatenate([att[:seqs], att[seqs:]], axis=1)

    ld_ow.wait()
    hp_full = dot(attended, ow[...]).astype(BF16)
    for q in range(NX):
        hp[q] = hp_full[:, q * quarter : (q + 1) * quarter]
    xfar = sorted(range(1, NX), key=lambda d: -min(d, NX - d))
    for d in xfar:
        xt = xplus(d)
        remote(hp.at[xt], hr.at[x], send.at[5], recv.at[5], {"tp": xt}).start()
    hr[pl.ds(x, 1)] = hp[pl.ds(x, 1)]
    own_tok = tok[:, pl.ds(pl.multiple_of(x * quarter, quarter), quarter)].astype(F32)
    wait_bytes(hr.at[pl.ds(0, NX - 1)], recv.at[5])
    residual = (own_tok + jnp.sum(hr[...].astype(F32), axis=0)).astype(BF16)

    stacked = jnp.concatenate([residual[:, q * HD : (q + 1) * HD] for q in range(QB)], axis=0)
    outgoing = dot(place, stacked, ((0,), (0,)))
    sb[...] = outgoing.reshape(NE, RB, HD).astype(BF16)
    for k in sorted(range(NZ), key=lambda d: -min(d, NZ - d)):
        zt = zplus(NZ - k)

        def send_one(i, carry, k=k, zt=zt):
            j, dev = pplus(i)
            remote(
                sb.at[zt * NP + j], xg.at[x, me], send.at[6], chunk_recv.at[k], {"ep_0": zt, **dev}
            ).start()
            return carry

        lax.fori_loop(0 if k else 1, NP, send_one, 0)
    xg[x, pl.ds(me, 1)] = sb[pl.ds(me, 1)]

    order = sorted(range(NZ), key=lambda d: (min(d, NZ - d), d))
    groups = [tuple(order[g : g + 2]) for g in range(0, NZ, 2)]
    for g, ks in enumerate(groups):
        for k in ks:
            zc = pl.multiple_of(zplus(k) * NP, NP)
            wait_bytes(xg.at[0, pl.ds(0, NP if k else NP - 1)], chunk_recv.at[k])
            for d in xfar:
                remote(
                    xg.at[x, pl.ds(zc, NP)], xg.at[x, pl.ds(zc, NP)],
                    send.at[7], group_recv.at[g], {"tp": xplus(d)},
                ).start()

    slots = 2 * NP * CAP
    pr = iota((QB * slots, QB * slots), 0)
    pc = iota((QB * slots, QB * slots), 1)
    to_q = ((lax.rem(pc, QB) == pr // slots) & (pc // QB == lax.rem(pr, slots))).astype(F32).astype(BF16)
    from_q = ((lax.rem(pr, QB) == pc // slots) & (pr // QB == lax.rem(pc, slots))).astype(F32).astype(BF16)
    ld_gf.wait()
    gain = gain_f[...]

    def experts(g):
        ks = groups[g]
        wait_bytes(xg.at[0, pl.ds(0, (NX - 1) * 2 * NP)], group_recv.at[g])
        blocks = []
        for q in range(NX):
            two = [
                xg[q, pl.ds(pl.multiple_of(zplus(k) * NP, NP), NP)].astype(F32).reshape(NP * RB, HD)
                for k in ks
            ]
            blocks.append(jnp.concatenate(two, axis=0))
        raw = jnp.concatenate(blocks, axis=1).astype(BF16)
        ordered = dot(to_q, raw)
        res = jnp.concatenate(
            [
                ordered[q * slots : (q + 1) * slots, a * HD : (a + 1) * HD]
                for a in range(NX)
                for q in range(QB)
            ],
            axis=1,
        )
        ffn_in = rms_scale(res, gain).astype(BF16)
        if g == 0:
            ld_gw.wait()
            ld_uw.wait()
            ld_dw.wait()
        gate_pre = dot(ffn_in, gw[...])
        upward = dot(ffn_in, uw[...])
        capped = jnp.minimum(gate_pre, clamp_limit)
        upward = jnp.clip(upward, -clamp_limit, clamp_limit)
        units = (capped * jax.nn.sigmoid(gate_alpha * capped) * (upward + 1.0)).astype(BF16)
        down = dot(units, dw[...]).astype(BF16)
        for q in range(NX):
            epart[g, q] = down[:, q * quarter : (q + 1) * quarter]
        for d in xfar:
            xt = xplus(d)
            remote(epart.at[g, xt], egot.at[g, x], send.at[8], group_got.at[g], {"tp": xt}).start()
        egot[g, pl.ds(x, 1)] = epart[g, pl.ds(x, 1)]

    def give_back(g):
        wait_bytes(egot.at[g, pl.ds(0, NX - 1)], group_got.at[g])
        summed = jnp.sum(egot[g].astype(F32), axis=0).astype(BF16)
        stack = jnp.concatenate([summed[:, q * HD : (q + 1) * HD] for q in range(QB)], axis=0)
        back = dot(from_q, stack).reshape(2 * NP, RB, HD).astype(BF16)
        for n, k in enumerate(groups[g]):
            zc = zplus(k)
            rb[pl.ds(pl.multiple_of(zc * NP, NP), NP)] = back[n * NP : (n + 1) * NP]
        for k in groups[g]:
            zc = zplus(k)

            def send_one(i, carry, zc=zc):
                j, dev = pplus(i)
                remote(
                    rb.at[zc * NP + j], rt.at[me], send.at[9], recv.at[9], {"ep_0": zc, **dev}
                ).start()
                return carry

            lax.fori_loop(0 if k else 1, NP, send_one, 0)
            if k == 0:
                rt[pl.ds(me, 1)] = rb[pl.ds(me, 1)]

    G = len(groups)
    experts(0)
    for g in range(1, G):
        experts(g)
        give_back(g - 1)
    give_back(G - 1)

    wait_bytes(got_kv.at[pl.ds(0, NZ - 1)], recv.at[4])
    kv = jnp.sum(got_kv[...].astype(F32), axis=0).astype(BF16)
    new_keys[...] = kv[:, :HD]
    new_values[...] = kv[:, HD:]

    wait_bytes(slices.at[pl.ds(0, NZ - 1)], send.at[0])
    wait_bytes(wq.at[pl.ds(0, NP - 1)], send.at[1])
    wait_bytes(wkv.at[pl.ds(0, NP - 1)], send.at[2])
    wait_bytes(got_q.at[pl.ds(0, NZ - 1)], send.at[3])
    wait_bytes(got_kv.at[pl.ds(0, NZ - 1)], send.at[4])
    wait_bytes(hr.at[pl.ds(0, NX - 1)], send.at[5])
    wait_bytes(xg.at[0, pl.ds(0, NE - 1)], send.at[6])
    wait_bytes(xg.at[pl.ds(0, NX - 1)], send.at[7])
    wait_bytes(egot.at[pl.ds(0, G * (NX - 1) // NX)], send.at[8])

    wait_bytes(rt.at[pl.ds(0, NE - 1)], recv.at[9])
    back = rt[...].astype(F32).reshape(NE * RB, HD).astype(BF16)
    routed = dot(weight_hi, back) + dot(weight_lo, back)
    res_f = residual.astype(F32)
    for q in range(QB):
        at = slice(q * HD, (q + 1) * HD)
        layer_out[:, at] = (res_f[:, at] + routed[q * seqs : (q + 1) * seqs]).astype(BF16)
    wait_bytes(rt.at[pl.ds(0, NE - 1)], send.at[9])


def body(
    tokens, key_cache, value_cache, lengths, attn_gain, query_weight, key_weight, value_weight,
    stay_bias, out_weight, ffn_gain, gate_weight, up_weight, down_weight, routes, route_weight,
):
    sizes = tuple(lax.axis_size(a) for a in AXES)
    NZ, NY, NC, NX = sizes
    NP, NE = NY * NC, NZ * NY * NC
    seqs, width = tokens.shape
    cache_len = key_cache.shape[1]
    quarter = width // NX
    kblock = width // NZ
    QB = quarter // HD
    RB = CAP * QB
    hidden = gate_weight.shape[2]
    G = NZ // 2
    slots = 2 * NP * CAP
    vm = pltpu.VMEM
    scratch = [
        vm((seqs, width), BF16), vm((1, width), F32), vm((1, width), F32),
        vm(routes.shape, jnp.int32), vm(route_weight.shape, F32),
        vm(key_cache.shape, BF16), vm(value_cache.shape, BF16),
        vm(out_weight.shape, BF16), vm((width, hidden), BF16), vm((width, hidden), BF16),
        vm((hidden, width), BF16),
        vm((seqs, width), BF16),
        vm((NZ, seqs, kblock), BF16),
        vm((NP, kblock // NP, 2 * HD), BF16), vm((NP, kblock // NP, 2 * HD), BF16),
        vm((NZ, seqs, 2 * HD), BF16), vm((NZ, seqs, 2 * HD), BF16),
        vm((NZ, seqs, 2 * HD), BF16), vm((NZ, seqs, 2 * HD), BF16),
        vm((2 * seqs, cache_len), BF16),
        vm((NX, seqs, quarter), BF16), vm((NX, seqs, quarter), BF16),
        vm((NE, RB, HD), BF16), vm((NX, NE, RB, HD), BF16),
        vm((G, NX, slots, quarter), BF16), vm((G, NX, slots, quarter), BF16),
        vm((NE, RB, HD), BF16), vm((NE, RB, HD), BF16),
        pltpu.SemaphoreType.DMA((8,)), pltpu.SemaphoreType.DMA((2, seqs // 2)),
        pltpu.SemaphoreType.DMA((4,)),
        pltpu.SemaphoreType.DMA((10,)), pltpu.SemaphoreType.DMA((10,)),
        pltpu.SemaphoreType.DMA((NZ,)), pltpu.SemaphoreType.DMA((G,)), pltpu.SemaphoreType.DMA((G,)),
    ]
    hbm = pl.BlockSpec(memory_space=pl.ANY)
    smem = pl.BlockSpec(memory_space=pltpu.SMEM)
    in_specs = [hbm] * 16
    in_specs[3] = smem
    in_specs[8] = smem
    out = [
        jax.ShapeDtypeStruct((seqs, quarter), BF16),
        jax.ShapeDtypeStruct((seqs, HD), BF16),
        jax.ShapeDtypeStruct((seqs, HD), BF16),
    ]
    return tuple(pl.pallas_call(
        functools.partial(layer_kernel, sizes),
        out_shape=out,
        in_specs=in_specs,
        out_specs=[pl.BlockSpec(memory_space=pltpu.VMEM)] * 3,
        scratch_shapes=scratch,
        compiler_params=pltpu.CompilerParams(
            collective_id=0, has_side_effects=True, vmem_limit_bytes=60 * 1024 * 1024
        ),
    )(
        tokens, key_cache, value_cache, lengths, attn_gain.reshape(1, width), query_weight,
        key_weight, value_weight, stay_bias, out_weight, ffn_gain.reshape(1, width), gate_weight,
        up_weight, down_weight, routes, route_weight,
    ))


def solution(mesh):
    finer = Mesh(mesh.devices.reshape(8, 4, 2, mesh.shape["tp"]), AXES)
    placed = (
        P(EP, None), P(EP, None, "tp"), P(EP, None, "tp"), P(EP), P(), P(EP, "tp"), P(EP, "tp"),
        P(EP, "tp"), P("tp"), P("tp", None), P(), P(EP, None, "tp"), P(EP, None, "tp"),
        P(EP, "tp", None), P(EP, None), P(EP, None),
    )
    return jax.shard_map(
        body, mesh=finer, in_specs=placed,
        out_specs=(P(EP, "tp"), P(EP, "tp"), P(EP, "tp")), check_vma=False,
    )
```

time: 175 us -> 65.7 us (0.38)
  Pallas kernels: 0 us -> 58.2 us
  waiting for transfers between devices: 49.4 us -> 0 us
  other arithmetic: 43.2 us -> 0 us
  blocking collectives: 32.9 us -> 0 us
  starting transfers between devices: 26.3 us -> 0 us
  matrix products: 11.6 us -> 0 us
  local copies, waits for them, and re-layouts: 10.1 us -> 6.57 us
    pallas_call x0 -> x1, Pallas kernels: none -> 58.2 us  [body(): pl.pallas_call(functools.partial(layer_kernel, sizes), out_shape=out, in_...]
    all_to_all x4 -> x0, waiting for transfers between devices: 49.4 us -> none  [the longest x2 31 us: copy_for_each(): return lax.all_to_all(copies, axis, split_axis=0, concat_axis=0, tiled=True)]
    another operation x3 -> x0, other arithmetic: 39.8 us -> none
    all_to_all x2 -> x0, blocking collectives: 32.9 us -> none  [the longest x1 25 us: body(): lax.all_to_all(outgoing, EP, split_axis=0, concat_axis=0, tiled=True)]
    all_to_all x4 -> x0, starting transfers between devices: 26.3 us -> none  [the longest x2 16 us: copy_for_each(): return lax.all_to_all(copies, axis, split_axis=0, concat_axis=0, tiled=True)]
    dot_general x9 -> x0, matrix products: 11.6 us -> none  [the longest x1 3.4 us: body(): jnp.einsum('skgd,sckd->skgc', grouped, key_rows, preferred_element_type=j...]
    unnamed x26 -> x5, local copies, waits for them, and re-layouts: 1.59 us -> 6.57 us
    convert_element_type x3 -> x0, local copies, waits for them, and re-layouts: 3.32 us -> none  [the longest x2 3.27 us: body(): partial_out.astype(jnp.bfloat16)]
  transfers between devices with their start and end apart: 4 -> 0, of which waited for: 4 -> 0; matrix products, arithmetic and copies ran while one was open for 2% -> 0% of each run, Pallas kernels for 0% -> 0%
where the time goes in v1:
time: 65.7 us; the launch traced here: 65.4 us
  Pallas kernels  58.2 us (89%)
  local copies, waits for them, and re-layouts  6.57 us (10%)
    pallas_call x1, Pallas kernels, body(): pl.pallas_call(functools.partial(layer_kernel, sizes), out_shape=out, in_...  58.2 us
    unnamed x5, local copies, waits for them, and re-layouts  6.57 us

profile of v1, /device:TPU:1, one launch (start us, length us, event | category | flops | bytes accessed | tf_op | source)
XLA Modules:
  0.0 65.4 jit_solution(4792940137779929619)
XLA Ops:
  0.6 1.4 %copy.19.routes = s32[16,4]{1,0:T(8,128)} copy(s32[16,4]{0,1:T(4,128)} %param.30) | data formatting | bytes 512 | tf_op args[14]
  2.0 1.3 %copy.20.route_weight = f32[16,4]{1,0:T(8,128)} copy(f32[16,4]{0,1:T(4,128)} %param.31) | data formatting | bytes 512 | tf_op args[15]
  3.3 58.2 %shard_map.175 = (bf16[16,512]{1,0:T(8,128)(2,1)}, bf16[16,128]{1,0:T(8,128)(2,1)}, bf16[16,128]{1,0:T(8,128)(2,1)}) custom-call(bf16[16,2048]{1,0:T(8,128)(2,1)} %tokens.1, bf16[16,1024,128]{2,1,0:T(8,128)(2,1)} %key_cache.1, bf16[16,1024,128]{2,1,0:T(8,128)(2,1)} %value_cache.1, s32[16]{0:T(128)} %lengths.1, f32[1,2048]{1,0:T(1,128)} %bitcast.2, ...), custom_call_target="tpu_custom_call" | custom-call | tf_op jit(solution)/shard_map/pallas_call | solution.py:402
  61.6 1.3 %copy.24 = bf16[16,512]{1,0:T(8,128)(2,1)} copy(bf16[16,512]{1,0:T(8,128)(2,1)} %get-tuple-element.6) | data formatting | bytes 32768
  62.9 1.3 %copy.25 = bf16[16,128]{1,0:T(8,128)(2,1)} copy(bf16[16,128]{1,0:T(8,128)(2,1)} %get-tuple-element.7) | data formatting | bytes 8192
  64.2 1.3 %copy.26 = bf16[16,128]{1,0:T(8,128)(2,1)} copy(bf16[16,128]{1,0:T(8,128)(2,1)} %get-tuple-element.8) | data formatting | bytes 8192

commit v2 on v1

--- a/solution.py
+++ b/solution.py
@@ -32,6 +32,10 @@
 
 def iota(shape, dim):
     return lax.broadcasted_iota(jnp.int32, shape, dim)
+
+
+def groups_of(near):
+    return [tuple(near[3:5]), tuple(near[5:]), tuple(near[:3])]
 
 
 def layer_kernel(
@@ -56,14 +60,18 @@
     QB = quarter // HD
     cache_len = kc.shape[1]
     RB = CAP * QB
-    topk = route_v.shape[1]
+    topk = route_v.shape[0]
 
     def zplus(d):
         return lax.rem(z + d, NZ)
 
+    plane = []
+    for i in range(NP):
+        j = lax.rem(yc + i, NP)
+        plane.append((j, {"ep_1": j // NC, "ep_2": lax.rem(j, NC)}))
+
     def pplus(i):
-        j = lax.rem(yc + i, NP)
-        return j, {"ep_1": j // NC, "ep_2": lax.rem(j, NC)}
+        return plane[i]
 
     def xplus(d):
         return lax.rem(x + d, NX)
@@ -144,17 +152,20 @@
     rows, cols = QB * seqs, NE * RB
     ld_rt.wait()
     ld_rw.wait()
-    route = jnp.concatenate([route_v[...]] * QB, axis=0)
-    rweight = jnp.concatenate([rweight_v[...]] * QB, axis=0)
     col = iota((rows, cols), 1)
     row = iota((rows, cols), 0)
-    col_e = col // RB
+    col_e = (col // RB).astype(F32)
+    diag = lax.rem(iota((rows, seqs), 0), seqs) == iota((rows, seqs), 1)
     hit = jnp.zeros((rows, cols), F32)
     weighted = jnp.zeros((rows, cols), F32)
+
+    def column(line):
+        return jnp.sum(jnp.where(diag, line, 0.0), axis=1, keepdims=True)
+
     for k in range(topk):
-        same = route[:, k : k + 1] == col_e
+        same = column(route_v[k : k + 1, :].astype(F32)) == col_e
         hit = jnp.where(same, 1.0, hit)
-        weighted = jnp.where(same, rweight[:, k : k + 1], weighted)
+        weighted = jnp.where(same, column(rweight_v[k : k + 1, :]), weighted)
     r0, r1 = iota((rows, rows), 0), iota((rows, rows), 1)
     earlier = ((r0 // seqs == r1 // seqs) & (r1 < r0)).astype(F32).astype(BF16)
     before = dot(earlier, hit.astype(BF16))
@@ -201,15 +212,18 @@
         carry = carry + within[:, 0:1]
     weights = sticks[...]
     att = jnp.zeros((2 * seqs, HD), F32)
-    for p in range(npair):
+    for p in range(0, npair, 2):
         ld_v[p].wait()
-        values = jnp.concatenate([vc[2 * p], vc[2 * p + 1]], axis=1)
-        mixed = dot(weights, values)
-        att = att + jnp.where(seq_of == 2 * p, mixed[:, :HD], 0.0)
-        att = att + jnp.where(seq_of == 2 * p + 1, mixed[:, HD:], 0.0)
+        ld_v[p + 1].wait()
+        four = range(2 * p, 2 * p + 4)
+        mixed = dot(weights, jnp.concatenate([vc[n] for n in four], axis=1))
+        for i, n in enumerate(four):
+            att = att + jnp.where(seq_of == n, mixed[:, i * HD : (i + 1) * HD], 0.0)
     att = att.astype(BF16)
     attended = jnp.concatenate([att[:seqs], att[seqs:]], axis=1)
 
+    near = sorted(range(NZ), key=lambda d: (min(d, NZ - d), d))
+    groups = groups_of(near)
     ld_ow.wait()
     hp_full = dot(attended, ow[...]).astype(BF16)
     for q in range(NX):
@@ -226,21 +240,15 @@
     stacked = jnp.concatenate([residual[:, q * HD : (q + 1) * HD] for q in range(QB)], axis=0)
     outgoing = dot(place, stacked, ((0,), (0,)))
     sb[...] = outgoing.reshape(NE, RB, HD).astype(BF16)
-    for k in sorted(range(NZ), key=lambda d: -min(d, NZ - d)):
+    for k in near:
         zt = zplus(NZ - k)
-
-        def send_one(i, carry, k=k, zt=zt):
+        for i in range(0 if k else 1, NP):
             j, dev = pplus(i)
             remote(
                 sb.at[zt * NP + j], xg.at[x, me], send.at[6], chunk_recv.at[k], {"ep_0": zt, **dev}
             ).start()
-            return carry
-
-        lax.fori_loop(0 if k else 1, NP, send_one, 0)
     xg[x, pl.ds(me, 1)] = sb[pl.ds(me, 1)]
 
-    order = sorted(range(NZ), key=lambda d: (min(d, NZ - d), d))
-    groups = [tuple(order[g : g + 2]) for g in range(0, NZ, 2)]
     for g, ks in enumerate(groups):
         for k in ks:
             zc = pl.multiple_of(zplus(k) * NP, NP)
@@ -251,33 +259,41 @@
                     send.at[7], group_recv.at[g], {"tp": xplus(d)},
                 ).start()
 
-    slots = 2 * NP * CAP
+    slots = NP * CAP
     pr = iota((QB * slots, QB * slots), 0)
     pc = iota((QB * slots, QB * slots), 1)
     to_q = ((lax.rem(pc, QB) == pr // slots) & (pc // QB == lax.rem(pr, slots))).astype(F32).astype(BF16)
     from_q = ((lax.rem(pr, QB) == pc // slots) & (pr // QB == lax.rem(pc, slots))).astype(F32).astype(BF16)
     ld_gf.wait()
     gain = gain_f[...]
+    starts = [slots * sum(len(ks) for ks in groups[:g]) for g in range(len(groups))]
 
     def experts(g):
         ks = groups[g]
-        wait_bytes(xg.at[0, pl.ds(0, (NX - 1) * 2 * NP)], group_recv.at[g])
-        blocks = []
-        for q in range(NX):
-            two = [
-                xg[q, pl.ds(pl.multiple_of(zplus(k) * NP, NP), NP)].astype(F32).reshape(NP * RB, HD)
+        at = pl.ds(starts[g], slots * len(ks))
+        wait_bytes(xg.at[pl.ds(0, NX - 1), pl.ds(0, len(ks) * NP)], group_recv.at[g])
+        raw = jnp.concatenate(
+            [
+                xg[a, pl.ds(pl.multiple_of(zplus(k) * NP, NP), NP)].astype(F32).reshape(NP * RB, HD)
                 for k in ks
-            ]
-            blocks.append(jnp.concatenate(two, axis=0))
-        raw = jnp.concatenate(blocks, axis=1).astype(BF16)
+                for a in range(NX)
+            ],
+            axis=1,
+        ).astype(BF16)
         ordered = dot(to_q, raw)
         res = jnp.concatenate(
             [
-                ordered[q * slots : (q + 1) * slots, a * HD : (a + 1) * HD]
-                for a in range(NX)
-                for q in range(QB)
+                jnp.concatenate(
+                    [
+                        ordered[q * slots : (q + 1) * slots, (n * NX + a) * HD : (n * NX + a + 1) * HD]
+                        for a in range(NX)
+                        for q in range(QB)
+                    ],
+                    axis=1,
+                )
+                for n in range(len(ks))
             ],
-            axis=1,
+            axis=0,
         )
         ffn_in = rms_scale(res, gain).astype(BF16)
         if g == 0:
@@ -291,31 +307,38 @@
         units = (capped * jax.nn.sigmoid(gate_alpha * capped) * (upward + 1.0)).astype(BF16)
         down = dot(units, dw[...]).astype(BF16)
         for q in range(NX):
-            epart[g, q] = down[:, q * quarter : (q + 1) * quarter]
+            epart[q, at] = down[:, q * quarter : (q + 1) * quarter]
         for d in xfar:
             xt = xplus(d)
-            remote(epart.at[g, xt], egot.at[g, x], send.at[8], group_got.at[g], {"tp": xt}).start()
-        egot[g, pl.ds(x, 1)] = epart[g, pl.ds(x, 1)]
+            remote(epart.at[xt, at], egot.at[x, at], send.at[8], group_got.at[g], {"tp": xt}).start()
+        egot[x, at] = epart[x, at]
 
     def give_back(g):
-        wait_bytes(egot.at[g, pl.ds(0, NX - 1)], group_got.at[g])
-        summed = jnp.sum(egot[g].astype(F32), axis=0).astype(BF16)
-        stack = jnp.concatenate([summed[:, q * HD : (q + 1) * HD] for q in range(QB)], axis=0)
-        back = dot(from_q, stack).reshape(2 * NP, RB, HD).astype(BF16)
-        for n, k in enumerate(groups[g]):
+        ks = groups[g]
+        at = pl.ds(starts[g], slots * len(ks))
+        wait_bytes(egot.at[pl.ds(0, NX - 1), at], group_got.at[g])
+        summed = jnp.sum(egot[:, at].astype(F32), axis=0).astype(BF16)
+        stack = jnp.concatenate(
+            [
+                jnp.concatenate(
+                    [summed[n * slots : (n + 1) * slots, q * HD : (q + 1) * HD] for q in range(QB)],
+                    axis=0,
+                )
+                for n in range(len(ks))
+            ],
+            axis=1,
+        )
+        back = dot(from_q, stack)
+        for n, k in enumerate(ks):
+            block = back[:, n * HD : (n + 1) * HD].reshape(NP, RB, HD).astype(BF16)
+            rb[pl.ds(pl.multiple_of(zplus(k) * NP, NP), NP)] = block
+        for k in ks:
             zc = zplus(k)
-            rb[pl.ds(pl.multiple_of(zc * NP, NP), NP)] = back[n * NP : (n + 1) * NP]
-        for k in groups[g]:
-            zc = zplus(k)
-
-            def send_one(i, carry, zc=zc):
+            for i in range(0 if k else 1, NP):
                 j, dev = pplus(i)
                 remote(
                     rb.at[zc * NP + j], rt.at[me], send.at[9], recv.at[9], {"ep_0": zc, **dev}
                 ).start()
-                return carry
-
-            lax.fori_loop(0 if k else 1, NP, send_one, 0)
             if k == 0:
                 rt[pl.ds(me, 1)] = rb[pl.ds(me, 1)]
 
@@ -339,7 +362,7 @@
     wait_bytes(hr.at[pl.ds(0, NX - 1)], send.at[5])
     wait_bytes(xg.at[0, pl.ds(0, NE - 1)], send.at[6])
     wait_bytes(xg.at[pl.ds(0, NX - 1)], send.at[7])
-    wait_bytes(egot.at[pl.ds(0, G * (NX - 1) // NX)], send.at[8])
+    wait_bytes(egot.at[pl.ds(0, NX - 1)], send.at[8])
 
     wait_bytes(rt.at[pl.ds(0, NE - 1)], recv.at[9])
     back = rt[...].astype(F32).reshape(NE * RB, HD).astype(BF16)
@@ -351,10 +374,17 @@
     wait_bytes(rt.at[pl.ds(0, NE - 1)], send.at[9])
 
 
+def tail_kernel(layer_in, keys_in, values_in, layer_out, new_keys, new_values):
+    layer_out[...] = layer_in[...]
+    new_keys[...] = keys_in[...]
+    new_values[...] = values_in[...]
+
+
 def body(
     tokens, key_cache, value_cache, lengths, attn_gain, query_weight, key_weight, value_weight,
     stay_bias, out_weight, ffn_gain, gate_weight, up_weight, down_weight, routes, route_weight,
 ):
+    routes, route_weight = routes.T, route_weight.T
     sizes = tuple(lax.axis_size(a) for a in AXES)
     NZ, NY, NC, NX = sizes
     NP, NE = NY * NC, NZ * NY * NC
@@ -365,8 +395,7 @@
     QB = quarter // HD
     RB = CAP * QB
     hidden = gate_weight.shape[2]
-    G = NZ // 2
-    slots = 2 * NP * CAP
+    G = len(groups_of(list(range(NZ))))
     vm = pltpu.VMEM
     scratch = [
         vm((seqs, width), BF16), vm((1, width), F32), vm((1, width), F32),
@@ -382,7 +411,7 @@
         vm((2 * seqs, cache_len), BF16),
         vm((NX, seqs, quarter), BF16), vm((NX, seqs, quarter), BF16),
         vm((NE, RB, HD), BF16), vm((NX, NE, RB, HD), BF16),
-        vm((G, NX, slots, quarter), BF16), vm((G, NX, slots, quarter), BF16),
+        vm((NX, NE * CAP, quarter), BF16), vm((NX, NE * CAP, quarter), BF16),
         vm((NE, RB, HD), BF16), vm((NE, RB, HD), BF16),
         pltpu.SemaphoreType.DMA((8,)), pltpu.SemaphoreType.DMA((2, seqs // 2)),
         pltpu.SemaphoreType.DMA((4,)),
@@ -399,7 +428,7 @@
         jax.ShapeDtypeStruct((seqs, HD), BF16),
         jax.ShapeDtypeStruct((seqs, HD), BF16),
     ]
-    return tuple(pl.pallas_call(
+    parts = pl.pallas_call(
         functools.partial(layer_kernel, sizes),
         out_shape=out,
         in_specs=in_specs,
@@ -412,7 +441,11 @@
         tokens, key_cache, value_cache, lengths, attn_gain.reshape(1, width), query_weight,
         key_weight, value_weight, stay_bias, out_weight, ffn_gain.reshape(1, width), gate_weight,
         up_weight, down_weight, routes, route_weight,
-    ))
+    )
+    vmem = pl.BlockSpec(memory_space=pltpu.VMEM)
+    return tuple(pl.pallas_call(
+        tail_kernel, out_shape=out, in_specs=[vmem] * 3, out_specs=[vmem] * 3,
+    )(*parts))
 
 
 def solution(mesh):

time: 65.7 us -> 56.4 us (0.86)
  local copies, waits for them, and re-layouts: 6.57 us -> 0 us
  Pallas kernels: 58.2 us -> 55.7 us
    unnamed x5 -> x0, local copies, waits for them, and re-layouts: 6.57 us -> none
    pallas_call x1, Pallas kernels: 58.2 us -> 54.3 us  [body(): pl.pallas_call(functools.partial(layer_kernel, sizes), out_shape=out, in_...]
    pallas_call x0 -> x1, Pallas kernels: none -> 1.34 us  [body(): pl.pallas_call(tail_kernel, out_shape=out, in_specs=[vmem] * 3, out_specs...]
where the time goes in v2:
time: 56.4 us; the launch traced here: 56.3 us
  Pallas kernels  55.7 us (99%)
  between operations  0.65 us (1%)
    pallas_call x1, Pallas kernels, body(): pl.pallas_call(functools.partial(layer_kernel, sizes), out_shape=out, in_...  54.3 us
    pallas_call x1, Pallas kernels, body(): pl.pallas_call(tail_kernel, out_shape=out, in_specs=[vmem] * 3, out_specs...  1.34 us

profile of v2, /device:TPU:1, one launch (start us, length us, event | category | flops | bytes accessed | tf_op | source)
XLA Modules:
  0.0 56.3 jit_solution(11156910892049113201)
XLA Ops:
  0.6 54.3 %shard_map.175 = (bf16[16,512]{1,0:T(8,128)(2,1)}, bf16[16,128]{1,0:T(8,128)(2,1)}, bf16[16,128]{1,0:T(8,128)(2,1)}) custom-call(bf16[16,2048]{1,0:T(8,128)(2,1)} %tokens.1, bf16[16,1024,128]{2,1,0:T(8,128)(2,1)} %key_cache.1, bf16[16,1024,128]{2,1,0:T(8,128)(2,1)} %value_cache.1, s32[16]{0:T(128)} %lengths.1, f32[1,2048]{1,0:T(1,128)} %bitcast.4, ...), custom_call_target="tpu_custom_call" | custom-call | tf_op jit(solution)/shard_map/pallas_call | solution.py:431
  55.0 1.3 %shard_map.176 = (bf16[16,512]{1,0:T(8,128)(2,1)}, bf16[16,128]{1,0:T(8,128)(2,1)}, bf16[16,128]{1,0:T(8,128)(2,1)}) custom-call(bf16[16,512]{1,0:T(8,128)(2,1)} %get-tuple-element.6.layer_in, bf16[16,128]{1,0:T(8,128)(2,1)} %get-tuple-element.7.keys_in, bf16[16,128]{1,0:T(8,128)(2,1)} %get-tuple-element.8.values_in), custom_call_target="tpu_custom_call" | custom-call | tf_op jit(solution)/shard_map/pallas_call | solution.py:446

commit v3 on v2

--- a/solution.py
+++ b/solution.py
@@ -20,30 +20,27 @@
 clamp_limit = 7.0
 gate_alpha = 1.702
 
-
 def dot(a, b, dims=((1,), (0,))):
     return lax.dot_general(a, b, (dims, ((), ())), preferred_element_type=F32)
-
 
 def rms_scale(values, gain):
     scale = lax.rsqrt(jnp.mean(values * values, axis=-1, keepdims=True) + eps_norm)
     return values * scale * gain
 
-
 def iota(shape, dim):
     return lax.broadcasted_iota(jnp.int32, shape, dim)
 
+DIRECT = 3
 
 def groups_of(near):
-    return [tuple(near[3:5]), tuple(near[5:]), tuple(near[:3])]
-
+    return [tuple(near[DIRECT:6]), tuple(near[6:])]
 
 def layer_kernel(
     sizes,
-    tokens, key_cache, value_cache, lengths, attn_gain, query_weight, key_weight, value_weight,
-    stay_bias, out_weight, ffn_gain, gate_weight, up_weight, down_weight, routes, route_weight,
+    tokens, key_cache, value_cache, lengths_in, attn_gain, query_weight, key_weight, value_weight,
+    bias_in, out_weight, ffn_gain, gate_weight, up_weight, down_weight, routes, route_weight,
     layer_out, new_keys, new_values,
-    tok, gain_a, gain_f, route_v, rweight_v, kc, vc, ow, gw, uw, dw,
+    resx, sbn, xn, rbn, rtn, nps, npr, lengths, stay_bias, tok, gain_a, gain_f, route_v, rweight_v, kc, vc, ow, gw, uw, dw,
     normed, slices, wq, wkv, part_q, part_kv, got_q, got_kv,
     sticks, hp, hr, sb, xg, epart, egot, rb, rt,
     loc, kv_sem, exp_sem, send, recv, chunk_recv, group_recv, group_got,
@@ -97,6 +94,8 @@
     ld_rt = load(routes, route_v, loc.at[5])
     ld_rw = load(route_weight, rweight_v, loc.at[6])
     ld_gf = load(ffn_gain, gain_f, loc.at[7])
+    ld_len = load(lengths_in, lengths, loc.at[8])
+    ld_bias = load(bias_in, stay_bias, loc.at[9])
     npair = seqs // 2
     ld_k = [load(key_cache.at[pl.ds(2 * p, 2)], kc.at[pl.ds(2 * p, 2)], kv_sem.at[0, p]) for p in range(npair)]
     ld_v = [load(value_cache.at[pl.ds(2 * p, 2)], vc.at[pl.ds(2 * p, 2)], kv_sem.at[1, p]) for p in range(npair)]
@@ -113,11 +112,14 @@
     def wait_bytes(ref, sem):
         pltpu.make_async_copy(ref, ref, sem).wait()
 
+
     ld_tok.wait()
     ld_ga.wait()
     normed[...] = rms_scale(tok[...].astype(F32), gain_a[...]).astype(BF16)
     ld_wq.wait()
+
     pl.semaphore_wait(barrier, NZ - 1 + NP - 1 + NX - 1)
+
     far = sorted(range(1, NZ), key=lambda d: -min(d, NZ - d))
     for d in far:
         zt = zplus(d)
@@ -133,21 +135,19 @@
         remote(wkv.at[yc], wkv.at[yc], send.at[2], recv.at[2], pplus(i)[1]).start()
     slices[pl.ds(z, 1)] = normed[:, pl.ds(pl.multiple_of(z * kblock, kblock), kblock)][None]
 
+    rt[...] = jnp.zeros_like(rt)
+    rtn[...] = jnp.zeros_like(rtn)
+
     wait_bytes(slices.at[pl.ds(0, NZ - 1)], recv.at[0])
+
     wait_bytes(wq.at[pl.ds(0, NP - 1)], recv.at[1])
+
     lhs = slices[...].reshape(NZ * seqs, kblock)
     part_q[...] = dot(lhs, wq[...].reshape(kblock, 2 * HD)).astype(BF16).reshape(NZ, seqs, 2 * HD)
     for d in far:
         zt = zplus(d)
         remote(part_q.at[zt], got_q.at[z], send.at[3], recv.at[3], {"ep_0": zt}).start()
     got_q[pl.ds(z, 1)] = part_q[pl.ds(z, 1)]
-
-    wait_bytes(wkv.at[pl.ds(0, NP - 1)], recv.at[2])
-    part_kv[...] = dot(lhs, wkv[...].reshape(kblock, 2 * HD)).astype(BF16).reshape(NZ, seqs, 2 * HD)
-    for d in far:
-        zt = zplus(d)
-        remote(part_kv.at[zt], got_kv.at[z], send.at[4], recv.at[4], {"ep_0": zt}).start()
-    got_kv[pl.ds(z, 1)] = part_kv[pl.ds(z, 1)]
 
     rows, cols = QB * seqs, NE * RB
     ld_rt.wait()
@@ -177,6 +177,8 @@
     weight_hi = weighted.astype(BF16)
     weight_lo = (weighted - weight_hi.astype(F32)).astype(BF16)
 
+    ld_len.wait()
+    ld_bias.wait()
     hrow = iota((2 * seqs, 1), 0)
     seq_of = lax.rem(hrow, seqs)
     length_col = jnp.zeros((2 * seqs, 1), jnp.int32)
@@ -185,17 +187,15 @@
     bias_col = jnp.where(hrow < seqs, stay_bias[0], stay_bias[1])
 
     wait_bytes(got_q.at[pl.ds(0, NZ - 1)], recv.at[3])
+
     query = jnp.sum(got_q[...].astype(F32), axis=0)
     query = jnp.concatenate([query[:, :HD], query[:, HD:]], axis=0).astype(BF16).astype(F32)
-    twice = jnp.concatenate([query, query], axis=1)
-    pair_row = lax.rem(iota((2 * seqs, 2 * HD), 0), seqs) - iota((2 * seqs, 2 * HD), 1) // HD
-    total = None
     for p in range(npair):
         ld_k[p].wait()
-        block = jnp.where(pair_row == 2 * p, twice, 0.0).astype(BF16)
-        keys = jnp.concatenate([kc[2 * p], kc[2 * p + 1]], axis=1)
-        term = dot(block, keys, ((1,), (1,)))
-        total = term if total is None else total + term
+    block = jnp.concatenate([jnp.where(seq_of == n, query, 0.0) for n in range(seqs)], axis=1)
+    keys = jnp.concatenate([kc[n] for n in range(seqs)], axis=1)
+    total = dot(block.astype(BF16), keys, ((1,), (1,)))
+
     zs = total * (HD ** -0.5) + bias_col
     live = iota((2 * seqs, cache_len), 1) < length_col
     log_stay = jnp.where(live, -(jnp.maximum(zs, 0.0) + jnp.log1p(jnp.exp(-jnp.abs(zs)))), 0.0)
@@ -210,49 +210,84 @@
         stick = jnp.where(live[:, at], jnp.exp(zs[:, at] + within + carry), 0.0)
         sticks[:, at] = stick.astype(BF16)
         carry = carry + within[:, 0:1]
+
     weights = sticks[...]
     att = jnp.zeros((2 * seqs, HD), F32)
-    for p in range(0, npair, 2):
+    for p in range(npair):
         ld_v[p].wait()
-        ld_v[p + 1].wait()
-        four = range(2 * p, 2 * p + 4)
-        mixed = dot(weights, jnp.concatenate([vc[n] for n in four], axis=1))
-        for i, n in enumerate(four):
-            att = att + jnp.where(seq_of == n, mixed[:, i * HD : (i + 1) * HD], 0.0)
+    mixed = dot(weights, jnp.concatenate([vc[n] for n in range(seqs)], axis=1))
+    for n in range(seqs):
+        att = att + jnp.where(seq_of == n, mixed[:, n * HD : (n + 1) * HD], 0.0)
     att = att.astype(BF16)
     attended = jnp.concatenate([att[:seqs], att[seqs:]], axis=1)
 
     near = sorted(range(NZ), key=lambda d: (min(d, NZ - d), d))
     groups = groups_of(near)
+    direct, far_ks = near[:DIRECT], [k for ks in groups for k in ks]
+
     ld_ow.wait()
+    xfar = sorted(range(1, NX), key=lambda d: -min(d, NX - d))
+
     hp_full = dot(attended, ow[...]).astype(BF16)
     for q in range(NX):
         hp[q] = hp_full[:, q * quarter : (q + 1) * quarter]
-    xfar = sorted(range(1, NX), key=lambda d: -min(d, NX - d))
+
     for d in xfar:
         xt = xplus(d)
         remote(hp.at[xt], hr.at[x], send.at[5], recv.at[5], {"tp": xt}).start()
     hr[pl.ds(x, 1)] = hp[pl.ds(x, 1)]
     own_tok = tok[:, pl.ds(pl.multiple_of(x * quarter, quarter), quarter)].astype(F32)
+
+    wait_bytes(wkv.at[pl.ds(0, NP - 1)], recv.at[2])
+
+    part_kv[...] = dot(lhs, wkv[...].reshape(kblock, 2 * HD)).astype(BF16).reshape(NZ, seqs, 2 * HD)
+    for d in far:
+        zt = zplus(d)
+        remote(part_kv.at[zt], got_kv.at[z], send.at[4], recv.at[4], {"ep_0": zt}).start()
+    got_kv[pl.ds(z, 1)] = part_kv[pl.ds(z, 1)]
+
     wait_bytes(hr.at[pl.ds(0, NX - 1)], recv.at[5])
+
     residual = (own_tok + jnp.sum(hr[...].astype(F32), axis=0)).astype(BF16)
 
+    resx[pl.ds(x, 1)] = residual[None]
     stacked = jnp.concatenate([residual[:, q * HD : (q + 1) * HD] for q in range(QB)], axis=0)
     outgoing = dot(place, stacked, ((0,), (0,)))
     sb[...] = outgoing.reshape(NE, RB, HD).astype(BF16)
-    for k in near:
+
+    for k in far_ks:
         zt = zplus(NZ - k)
-        for i in range(0 if k else 1, NP):
+        for i in range(NP):
             j, dev = pplus(i)
             remote(
                 sb.at[zt * NP + j], xg.at[x, me], send.at[6], chunk_recv.at[k], {"ep_0": zt, **dev}
             ).start()
-    xg[x, pl.ds(me, 1)] = sb[pl.ds(me, 1)]
+    for d in xfar:
+        remote(resx.at[x], resx.at[x], send.at[10], recv.at[10], {"tp": xplus(d)}).start()
+
+    wait_bytes(resx.at[pl.ds(0, NX - 1)], recv.at[10])
+
+    stacked = jnp.concatenate(
+        [
+            jnp.concatenate([resx[a, :, q * HD : (q + 1) * HD] for a in range(NX)], axis=1)
+            for q in range(QB)
+        ],
+        axis=0,
+    )
+    sbn[...] = dot(place, stacked, ((0,), (0,))).reshape(NE, RB, NX * HD).astype(BF16)
+
+    for k in direct:
+        zt = zplus(NZ - k)
+        for i in range(0 if k else 1, NP):
+            j, dev = pplus(i)
+            remote(sbn.at[zt * NP + j], xn.at[me], send.at[11], recv.at[11], {"ep_0": zt, **dev}).start()
+    xn[pl.ds(me, 1)] = sbn[pl.ds(me, 1)]
 
     for g, ks in enumerate(groups):
         for k in ks:
+
             zc = pl.multiple_of(zplus(k) * NP, NP)
-            wait_bytes(xg.at[0, pl.ds(0, NP if k else NP - 1)], chunk_recv.at[k])
+            wait_bytes(xg.at[0, pl.ds(0, NP)], chunk_recv.at[k])
             for d in xfar:
                 remote(
                     xg.at[x, pl.ds(zc, NP)], xg.at[x, pl.ds(zc, NP)],
@@ -265,21 +300,14 @@
     to_q = ((lax.rem(pc, QB) == pr // slots) & (pc // QB == lax.rem(pr, slots))).astype(F32).astype(BF16)
     from_q = ((lax.rem(pr, QB) == pc // slots) & (pr // QB == lax.rem(pc, slots))).astype(F32).astype(BF16)
     ld_gf.wait()
+    ld_gw.wait()
+    ld_uw.wait()
+    ld_dw.wait()
     gain = gain_f[...]
     starts = [slots * sum(len(ks) for ks in groups[:g]) for g in range(len(groups))]
 
-    def experts(g):
-        ks = groups[g]
-        at = pl.ds(starts[g], slots * len(ks))
-        wait_bytes(xg.at[pl.ds(0, NX - 1), pl.ds(0, len(ks) * NP)], group_recv.at[g])
-        raw = jnp.concatenate(
-            [
-                xg[a, pl.ds(pl.multiple_of(zplus(k) * NP, NP), NP)].astype(F32).reshape(NP * RB, HD)
-                for k in ks
-                for a in range(NX)
-            ],
-            axis=1,
-        ).astype(BF16)
+    def expert_rows(raw):
+        chunks = raw.shape[1] // (NX * HD)
         ordered = dot(to_q, raw)
         res = jnp.concatenate(
             [
@@ -291,23 +319,88 @@
                     ],
                     axis=1,
                 )
-                for n in range(len(ks))
+                for n in range(chunks)
             ],
             axis=0,
         )
         ffn_in = rms_scale(res, gain).astype(BF16)
-        if g == 0:
-            ld_gw.wait()
-            ld_uw.wait()
-            ld_dw.wait()
         gate_pre = dot(ffn_in, gw[...])
         upward = dot(ffn_in, uw[...])
         capped = jnp.minimum(gate_pre, clamp_limit)
         upward = jnp.clip(upward, -clamp_limit, clamp_limit)
         units = (capped * jax.nn.sigmoid(gate_alpha * capped) * (upward + 1.0)).astype(BF16)
-        down = dot(units, dw[...]).astype(BF16)
+        return units
+
+    def sources(k):
+        return pl.ds(pl.multiple_of(zplus(k) * NP, NP), NP)
+
+    def near_experts():
+
+        wait_bytes(xn.at[pl.ds(0, len(direct) * NP - 1)], recv.at[11])
+
+        raw = jnp.concatenate(
+            [xn[sources(k)].astype(F32).reshape(NP * RB, NX * HD) for k in direct], axis=1
+        ).astype(BF16)
+        down = dot(expert_rows(raw), dw[...]).astype(BF16)
+        stack = jnp.concatenate(
+            [
+                jnp.concatenate(
+                    [
+                        down[n * slots : (n + 1) * slots, a * quarter + q * HD : a * quarter + (q + 1) * HD]
+                        for n in range(len(direct))
+                        for a in range(NX)
+                    ],
+                    axis=1,
+                )
+                for q in range(QB)
+            ],
+            axis=0,
+        )
+        back = dot(from_q, stack)
+        for n, k in enumerate(direct):
+            block = back[:, n * NX * HD : (n + 1) * NX * HD].reshape(NP, RB, NX * HD)
+            rbn[sources(k)] = block.astype(BF16)
+
+        for k in direct:
+            zc = zplus(k)
+            for i in range(0 if k else 1, NP):
+                j, dev = pplus(i)
+                remote(
+                    rbn.at[zc * NP + j], rtn.at[me], send.at[12], recv.at[12], {"ep_0": zc, **dev}
+                ).start()
+        rtn[pl.ds(me, 1)] = rbn[pl.ds(me, 1)]
+
+    def near_combine():
+
+        wait_bytes(rtn.at[pl.ds(0, len(direct) * NP - 1)], recv.at[12])
+
+        back = rtn[...].astype(F32).reshape(NE * RB, NX * HD).astype(BF16)
+        mine = (dot(weight_hi, back) + dot(weight_lo, back)).astype(BF16)
+        for a in range(NX):
+            nps[a] = mine[:, a * HD : (a + 1) * HD]
+        for d in xfar:
+            xt = xplus(d)
+            remote(nps.at[xt], npr.at[x], send.at[13], recv.at[13], {"tp": xt}).start()
+        npr[pl.ds(x, 1)] = nps[pl.ds(x, 1)]
+
+    def experts(g):
+        ks = groups[g]
+        at = pl.ds(starts[g], slots * len(ks))
+
+        wait_bytes(xg.at[pl.ds(0, NX - 1), pl.ds(0, len(ks) * NP)], group_recv.at[g])
+
+        raw = jnp.concatenate(
+            [
+                xg[a, sources(k)].astype(F32).reshape(NP * RB, HD)
+                for k in ks
+                for a in range(NX)
+            ],
+            axis=1,
+        ).astype(BF16)
+        down = dot(expert_rows(raw), dw[...]).astype(BF16)
         for q in range(NX):
             epart[q, at] = down[:, q * quarter : (q + 1) * quarter]
+
         for d in xfar:
             xt = xplus(d)
             remote(epart.at[xt, at], egot.at[x, at], send.at[8], group_got.at[g], {"tp": xt}).start()
@@ -316,38 +409,39 @@
     def give_back(g):
         ks = groups[g]
         at = pl.ds(starts[g], slots * len(ks))
+
         wait_bytes(egot.at[pl.ds(0, NX - 1), at], group_got.at[g])
+
         summed = jnp.sum(egot[:, at].astype(F32), axis=0).astype(BF16)
         stack = jnp.concatenate(
             [
                 jnp.concatenate(
-                    [summed[n * slots : (n + 1) * slots, q * HD : (q + 1) * HD] for q in range(QB)],
-                    axis=0,
+                    [summed[n * slots : (n + 1) * slots, q * HD : (q + 1) * HD] for n in range(len(ks))],
+                    axis=1,
                 )
-                for n in range(len(ks))
+                for q in range(QB)
             ],
-            axis=1,
+            axis=0,
         )
         back = dot(from_q, stack)
         for n, k in enumerate(ks):
-            block = back[:, n * HD : (n + 1) * HD].reshape(NP, RB, HD).astype(BF16)
-            rb[pl.ds(pl.multiple_of(zplus(k) * NP, NP), NP)] = block
+            rb[sources(k)] = back[:, n * HD : (n + 1) * HD].reshape(NP, RB, HD).astype(BF16)
+
         for k in ks:
             zc = zplus(k)
-            for i in range(0 if k else 1, NP):
+            for i in range(NP):
                 j, dev = pplus(i)
                 remote(
                     rb.at[zc * NP + j], rt.at[me], send.at[9], recv.at[9], {"ep_0": zc, **dev}
                 ).start()
-            if k == 0:
-                rt[pl.ds(me, 1)] = rb[pl.ds(me, 1)]
 
     G = len(groups)
-    experts(0)
-    for g in range(1, G):
+    for g in range(G):
         experts(g)
-        give_back(g - 1)
-    give_back(G - 1)
+    near_experts()
+    for g in range(G):
+        give_back(g)
+    near_combine()
 
     wait_bytes(got_kv.at[pl.ds(0, NZ - 1)], recv.at[4])
     kv = jnp.sum(got_kv[...].astype(F32), axis=0).astype(BF16)
@@ -360,25 +454,34 @@
     wait_bytes(got_q.at[pl.ds(0, NZ - 1)], send.at[3])
     wait_bytes(got_kv.at[pl.ds(0, NZ - 1)], send.at[4])
     wait_bytes(hr.at[pl.ds(0, NX - 1)], send.at[5])
-    wait_bytes(xg.at[0, pl.ds(0, NE - 1)], send.at[6])
-    wait_bytes(xg.at[pl.ds(0, NX - 1)], send.at[7])
-    wait_bytes(egot.at[pl.ds(0, NX - 1)], send.at[8])
-
-    wait_bytes(rt.at[pl.ds(0, NE - 1)], recv.at[9])
+    far_blocks = len(far_ks) * NP
+    near_blocks = len(direct) * NP - 1
+    wait_bytes(xg.at[0, pl.ds(0, far_blocks)], send.at[6])
+    wait_bytes(xg.at[pl.ds(0, NX - 1), pl.ds(0, far_blocks)], send.at[7])
+    wait_bytes(egot.at[pl.ds(0, NX - 1), pl.ds(0, far_blocks * CAP)], send.at[8])
+    wait_bytes(resx.at[pl.ds(0, NX - 1)], send.at[10])
+    wait_bytes(xn.at[pl.ds(0, near_blocks)], send.at[11])
+    wait_bytes(rtn.at[pl.ds(0, near_blocks)], send.at[12])
+    wait_bytes(npr.at[pl.ds(0, NX - 1)], send.at[13])
+
+    wait_bytes(npr.at[pl.ds(0, NX - 1)], recv.at[13])
+    near_sum = jnp.sum(npr[...].astype(F32), axis=0)
+
+    wait_bytes(rt.at[pl.ds(0, far_blocks)], recv.at[9])
+
     back = rt[...].astype(F32).reshape(NE * RB, HD).astype(BF16)
-    routed = dot(weight_hi, back) + dot(weight_lo, back)
+    routed = near_sum + dot(weight_hi, back) + dot(weight_lo, back)
     res_f = residual.astype(F32)
     for q in range(QB):
         at = slice(q * HD, (q + 1) * HD)
         layer_out[:, at] = (res_f[:, at] + routed[q * seqs : (q + 1) * seqs]).astype(BF16)
-    wait_bytes(rt.at[pl.ds(0, NE - 1)], send.at[9])
-
+
+    wait_bytes(rt.at[pl.ds(0, far_blocks)], send.at[9])
 
 def tail_kernel(layer_in, keys_in, values_in, layer_out, new_keys, new_values):
     layer_out[...] = layer_in[...]
     new_keys[...] = keys_in[...]
     new_values[...] = values_in[...]
-
 
 def body(
     tokens, key_cache, value_cache, lengths, attn_gain, query_weight, key_weight, value_weight,
@@ -398,6 +501,10 @@
     G = len(groups_of(list(range(NZ))))
     vm = pltpu.VMEM
     scratch = [
+        vm((NX, seqs, quarter), BF16),
+        *[vm((NE, RB, NX * HD), BF16)] * 4,
+        *[vm((NX, QB * seqs, HD), BF16)] * 2,
+        pltpu.SMEM(lengths.shape, jnp.int32), pltpu.SMEM(stay_bias.shape, F32),
         vm((seqs, width), BF16), vm((1, width), F32), vm((1, width), F32),
         vm(routes.shape, jnp.int32), vm(route_weight.shape, F32),
         vm(key_cache.shape, BF16), vm(value_cache.shape, BF16),
@@ -413,24 +520,18 @@
         vm((NE, RB, HD), BF16), vm((NX, NE, RB, HD), BF16),
         vm((NX, NE * CAP, quarter), BF16), vm((NX, NE * CAP, quarter), BF16),
         vm((NE, RB, HD), BF16), vm((NE, RB, HD), BF16),
-        pltpu.SemaphoreType.DMA((8,)), pltpu.SemaphoreType.DMA((2, seqs // 2)),
+        pltpu.SemaphoreType.DMA((10,)), pltpu.SemaphoreType.DMA((2, seqs // 2)),
         pltpu.SemaphoreType.DMA((4,)),
-        pltpu.SemaphoreType.DMA((10,)), pltpu.SemaphoreType.DMA((10,)),
+        pltpu.SemaphoreType.DMA((14,)), pltpu.SemaphoreType.DMA((14,)),
         pltpu.SemaphoreType.DMA((NZ,)), pltpu.SemaphoreType.DMA((G,)), pltpu.SemaphoreType.DMA((G,)),
     ]
     hbm = pl.BlockSpec(memory_space=pl.ANY)
-    smem = pl.BlockSpec(memory_space=pltpu.SMEM)
     in_specs = [hbm] * 16
-    in_specs[3] = smem
-    in_specs[8] = smem
-    out = [
-        jax.ShapeDtypeStruct((seqs, quarter), BF16),
-        jax.ShapeDtypeStruct((seqs, HD), BF16),
-        jax.ShapeDtypeStruct((seqs, HD), BF16),
-    ]
+    shapes = [(seqs, quarter), (seqs, HD), (seqs, HD)]
+    out = [jax.ShapeDtypeStruct(shape, BF16) for shape in shapes]
     parts = pl.pallas_call(
         functools.partial(layer_kernel, sizes),
-        out_shape=out,
+        out_shape=[pltpu.VMEM(shape, BF16) for shape in shapes],
         in_specs=in_specs,
         out_specs=[pl.BlockSpec(memory_space=pltpu.VMEM)] * 3,
         scratch_shapes=scratch,
@@ -445,8 +546,8 @@
     vmem = pl.BlockSpec(memory_space=pltpu.VMEM)
     return tuple(pl.pallas_call(
         tail_kernel, out_shape=out, in_specs=[vmem] * 3, out_specs=[vmem] * 3,
+        compiler_params=pltpu.CompilerParams(vmem_limit_bytes=1024 * 1024),
     )(*parts))
-
 
 def solution(mesh):
     finer = Mesh(mesh.devices.reshape(8, 4, 2, mesh.shape["tp"]), AXES)

time: 56.4 us -> 50.9 us (0.902)
  Pallas kernels: 55.7 us -> 50.2 us
    pallas_call x1, Pallas kernels: 54.3 us -> 49.6 us  [body(): pl.pallas_call(functools.partial(layer_kernel, sizes), out_shape=[pltpu.V...]
    pallas_call x1, Pallas kernels: 1.34 us -> 0.61 us  [body(): pl.pallas_call(tail_kernel, out_shape=out, in_specs=[vmem] * 3, out_specs...]
where the time goes in v3:
time: 50.9 us
  Pallas kernels  50.2 us (99%)
  between operations  0.65 us (1%)
    pallas_call x1, Pallas kernels, body(): pl.pallas_call(functools.partial(layer_kernel, sizes), out_shape=[pltpu.V...  49.6 us

profile of v3, /device:TPU:1, one launch (start us, length us, event | category | flops | bytes accessed | tf_op | source)
XLA Modules:
  0.0 50.9 jit_solution(15720153209034491267)
XLA Ops:
  0.6 49.6 %shard_map.175 = (bf16[16,512]{1,0:T(8,128)(2,1)S(1)}, bf16[16,128]{1,0:T(8,128)(2,1)S(1)}, bf16[16,128]{1,0:T(8,128)(2,1)S(1)}) custom-call(bf16[16,2048]{1,0:T(8,128)(2,1)} %tokens.1, bf16[16,1024,128]{2,1,0:T(8,128)(2,1)} %key_cache.1, bf16[16,1024,128]{2,1,0:T(8,128)(2,1)} %value_cache.1, s32[16]{0:T(128)} %lengths_in.1, f32[1,2048]{1,0:T(1,128)} %bitcast.4, ...), custom_call_target="tpu_custom_call" | custom-call | tf_op jit(solution)/shard_map/pallas_call | solution.py:532
  50.2 0.6 %shard_map.176 = (bf16[16,512]{1,0:T(8,128)(2,1)}, bf16[16,128]{1,0:T(8,128)(2,1)}, bf16[16,128]{1,0:T(8,128)(2,1)}) custom-call(bf16[16,512]{1,0:T(8,128)(2,1)S(1)} %get-tuple-element.6.layer_in, bf16[16,128]{1,0:T(8,128)(2,1)S(1)} %get-tuple-element.7.keys_in, bf16[16,128]{1,0:T(8,128)(2,1)S(1)} %get-tuple-element.8.values_in), custom_call_target="tpu_custom_call" | custom-call | tf_op jit(solution)/shard_map/pallas_call | solution.py:547

commit v4 on v3

--- a/solution.py
+++ b/solution.py
@@ -30,17 +30,17 @@
 def iota(shape, dim):
     return lax.broadcasted_iota(jnp.int32, shape, dim)
 
-DIRECT = 3
+DIRECT = 5
 
 def groups_of(near):
-    return [tuple(near[DIRECT:6]), tuple(near[6:])]
+    return [tuple(near[7:]), tuple(near[DIRECT:7])]
 
 def layer_kernel(
     sizes,
     tokens, key_cache, value_cache, lengths_in, attn_gain, query_weight, key_weight, value_weight,
     bias_in, out_weight, ffn_gain, gate_weight, up_weight, down_weight, routes, route_weight,
     layer_out, new_keys, new_values,
-    resx, sbn, xn, rbn, rtn, nps, npr, lengths, stay_bias, tok, gain_a, gain_f, route_v, rweight_v, kc, vc, ow, gw, uw, dw,
+    sbn, xn, rbn, rtn, nps, npr, lengths, stay_bias, tok, gain_a, gain_f, route_v, rweight_v, kc, kt, vc, ow, guw, dw,
     normed, slices, wq, wkv, part_q, part_kv, got_q, got_kv,
     sticks, hp, hr, sb, xg, epart, egot, rb, rt,
     loc, kv_sem, exp_sem, send, recv, chunk_recv, group_recv, group_got,
@@ -100,8 +100,9 @@
     ld_k = [load(key_cache.at[pl.ds(2 * p, 2)], kc.at[pl.ds(2 * p, 2)], kv_sem.at[0, p]) for p in range(npair)]
     ld_v = [load(value_cache.at[pl.ds(2 * p, 2)], vc.at[pl.ds(2 * p, 2)], kv_sem.at[1, p]) for p in range(npair)]
     ld_ow = load(out_weight, ow, exp_sem.at[0])
-    ld_gw = load(gate_weight.at[0], gw, exp_sem.at[1])
-    ld_uw = load(up_weight.at[0], uw, exp_sem.at[2])
+    hidden = dw.shape[0]
+    ld_gw = load(gate_weight.at[0], guw.at[:, pl.ds(0, hidden)], exp_sem.at[1])
+    ld_uw = load(up_weight.at[0], guw.at[:, pl.ds(hidden, hidden)], exp_sem.at[2])
     ld_dw = load(down_weight.at[0], dw, exp_sem.at[3])
 
     def remote(src, dst, s, r, device):
@@ -138,6 +139,14 @@
     rt[...] = jnp.zeros_like(rt)
     rtn[...] = jnp.zeros_like(rtn)
 
+    def transpose_keys(pairs):
+        for p in pairs:
+            ld_k[p].wait()
+            for s in (2 * p, 2 * p + 1):
+                kt[s] = kc[s].T
+
+    transpose_keys(range(npair // 2))
+
     wait_bytes(slices.at[pl.ds(0, NZ - 1)], recv.at[0])
 
     wait_bytes(wq.at[pl.ds(0, NP - 1)], recv.at[1])
@@ -186,30 +195,41 @@
         length_col = jnp.where(seq_of == s, lengths[s], length_col)
     bias_col = jnp.where(hrow < seqs, stay_bias[0], stay_bias[1])
 
+    transpose_keys(range(npair // 2, npair))
+
     wait_bytes(got_q.at[pl.ds(0, NZ - 1)], recv.at[3])
 
     query = jnp.sum(got_q[...].astype(F32), axis=0)
     query = jnp.concatenate([query[:, :HD], query[:, HD:]], axis=0).astype(BF16).astype(F32)
-    for p in range(npair):
-        ld_k[p].wait()
     block = jnp.concatenate([jnp.where(seq_of == n, query, 0.0) for n in range(seqs)], axis=1)
-    keys = jnp.concatenate([kc[n] for n in range(seqs)], axis=1)
-    total = dot(block.astype(BF16), keys, ((1,), (1,)))
+    total = dot(block.astype(BF16), kt[...].reshape(seqs * HD, cache_len))
 
     zs = total * (HD ** -0.5) + bias_col
     live = iota((2 * seqs, cache_len), 1) < length_col
     log_stay = jnp.where(live, -(jnp.maximum(zs, 0.0) + jnp.log1p(jnp.exp(-jnp.abs(zs)))), 0.0)
-    hi = log_stay.astype(BF16)
-    lo = (log_stay - hi.astype(F32)).astype(BF16)
     blk = min(256, cache_len)
+    nblk = cache_len // blk
+    n = 2 * seqs
+    parts = [log_stay[:, b * blk : (b + 1) * blk] for b in range(nblk)]
+    after = [None] * nblk
+    for b in reversed(range(nblk - 1)):
+        after[b] = parts[b + 1] if after[b + 1] is None else parts[b + 1] + after[b + 1]
+
+    def summed_by(matrix, terms):
+        terms = jnp.concatenate(terms, axis=0)
+        hi = terms.astype(BF16)
+        lo = (terms - hi.astype(F32)).astype(BF16)
+        return dot(hi, matrix) + dot(lo, matrix)
+
     tri = (iota((blk, blk), 0) >= iota((blk, blk), 1)).astype(F32).astype(BF16)
-    carry = jnp.zeros((2 * seqs, 1), F32)
-    for b in reversed(range(cache_len // blk)):
+    from_here = summed_by(tri, parts)
+    from_later = summed_by(jnp.ones((blk, blk), BF16), after[:-1]) if nblk > 1 else None
+    for b in range(nblk):
         at = slice(b * blk, (b + 1) * blk)
-        within = dot(hi[:, at], tri) + dot(lo[:, at], tri)
-        stick = jnp.where(live[:, at], jnp.exp(zs[:, at] + within + carry), 0.0)
-        sticks[:, at] = stick.astype(BF16)
-        carry = carry + within[:, 0:1]
+        power = zs[:, at] + from_here[b * n : (b + 1) * n]
+        if b < nblk - 1:
+            power = power + from_later[b * n : (b + 1) * n]
+        sticks[:, at] = jnp.where(live[:, at], jnp.exp(power), 0.0).astype(BF16)
 
     weights = sticks[...]
     att = jnp.zeros((2 * seqs, HD), F32)
@@ -234,8 +254,12 @@
 
     for d in xfar:
         xt = xplus(d)
-        remote(hp.at[xt], hr.at[x], send.at[5], recv.at[5], {"tp": xt}).start()
-    hr[pl.ds(x, 1)] = hp[pl.ds(x, 1)]
+        remote(hp.at[xt], hr.at[x, xt], send.at[5], recv.at[5], {"tp": xt}).start()
+    for n in range(1, NX):
+        for d in xfar:
+            xt, q = xplus(d), xplus(d + n)
+            remote(hp.at[q], hr.at[x, q], send.at[10], recv.at[10], {"tp": xt}).start()
+    hr[pl.ds(x, 1)] = hp[...][None]
     own_tok = tok[:, pl.ds(pl.multiple_of(x * quarter, quarter), quarter)].astype(F32)
 
     wait_bytes(wkv.at[pl.ds(0, NP - 1)], recv.at[2])
@@ -246,11 +270,10 @@
         remote(part_kv.at[zt], got_kv.at[z], send.at[4], recv.at[4], {"ep_0": zt}).start()
     got_kv[pl.ds(z, 1)] = part_kv[pl.ds(z, 1)]
 
-    wait_bytes(hr.at[pl.ds(0, NX - 1)], recv.at[5])
-
-    residual = (own_tok + jnp.sum(hr[...].astype(F32), axis=0)).astype(BF16)
-
-    resx[pl.ds(x, 1)] = residual[None]
+    wait_bytes(hr.at[0, pl.ds(0, NX - 1)], recv.at[5])
+
+    residual = (own_tok + jnp.sum(hr[:, pl.ds(x, 1)].astype(F32), axis=(0, 1))).astype(BF16)
+
     stacked = jnp.concatenate([residual[:, q * HD : (q + 1) * HD] for q in range(QB)], axis=0)
     outgoing = dot(place, stacked, ((0,), (0,)))
     sb[...] = outgoing.reshape(NE, RB, HD).astype(BF16)
@@ -262,21 +285,25 @@
             remote(
                 sb.at[zt * NP + j], xg.at[x, me], send.at[6], chunk_recv.at[k], {"ep_0": zt, **dev}
             ).start()
-    for d in xfar:
-        remote(resx.at[x], resx.at[x], send.at[10], recv.at[10], {"tp": xplus(d)}).start()
-
-    wait_bytes(resx.at[pl.ds(0, NX - 1)], recv.at[10])
-
+
+    wait_bytes(hr.at[pl.ds(0, NX - 1), pl.ds(0, NX - 1)], recv.at[10])
+
+    rows_of = [
+        (
+            tok[:, a * quarter : (a + 1) * quarter].astype(F32) + jnp.sum(hr[:, a].astype(F32), axis=0)
+        ).astype(BF16)
+        for a in range(NX)
+    ]
     stacked = jnp.concatenate(
         [
-            jnp.concatenate([resx[a, :, q * HD : (q + 1) * HD] for a in range(NX)], axis=1)
+            jnp.concatenate([rows_of[a][:, q * HD : (q + 1) * HD] for a in range(NX)], axis=1)
             for q in range(QB)
         ],
         axis=0,
     )
     sbn[...] = dot(place, stacked, ((0,), (0,))).reshape(NE, RB, NX * HD).astype(BF16)
 
-    for k in direct:
+    for k in direct[::-1]:
         zt = zplus(NZ - k)
         for i in range(0 if k else 1, NP):
             j, dev = pplus(i)
@@ -324,10 +351,9 @@
             axis=0,
         )
         ffn_in = rms_scale(res, gain).astype(BF16)
-        gate_pre = dot(ffn_in, gw[...])
-        upward = dot(ffn_in, uw[...])
-        capped = jnp.minimum(gate_pre, clamp_limit)
-        upward = jnp.clip(upward, -clamp_limit, clamp_limit)
+        both = dot(ffn_in, guw[...])
+        capped = jnp.minimum(both[:, :hidden], clamp_limit)
+        upward = jnp.clip(both[:, hidden:], -clamp_limit, clamp_limit)
         units = (capped * jax.nn.sigmoid(gate_alpha * capped) * (upward + 1.0)).astype(BF16)
         return units
 
@@ -361,7 +387,7 @@
             block = back[:, n * NX * HD : (n + 1) * NX * HD].reshape(NP, RB, NX * HD)
             rbn[sources(k)] = block.astype(BF16)
 
-        for k in direct:
+        for k in direct[::-1]:
             zc = zplus(k)
             for i in range(0 if k else 1, NP):
                 j, dev = pplus(i)
@@ -436,9 +462,9 @@
                 ).start()
 
     G = len(groups)
+    near_experts()
     for g in range(G):
         experts(g)
-    near_experts()
     for g in range(G):
         give_back(g)
     near_combine()
@@ -453,13 +479,13 @@
     wait_bytes(wkv.at[pl.ds(0, NP - 1)], send.at[2])
     wait_bytes(got_q.at[pl.ds(0, NZ - 1)], send.at[3])
     wait_bytes(got_kv.at[pl.ds(0, NZ - 1)], send.at[4])
-    wait_bytes(hr.at[pl.ds(0, NX - 1)], send.at[5])
+    wait_bytes(hr.at[0, pl.ds(0, NX - 1)], send.at[5])
     far_blocks = len(far_ks) * NP
     near_blocks = len(direct) * NP - 1
     wait_bytes(xg.at[0, pl.ds(0, far_blocks)], send.at[6])
     wait_bytes(xg.at[pl.ds(0, NX - 1), pl.ds(0, far_blocks)], send.at[7])
     wait_bytes(egot.at[pl.ds(0, NX - 1), pl.ds(0, far_blocks * CAP)], send.at[8])
-    wait_bytes(resx.at[pl.ds(0, NX - 1)], send.at[10])
+    wait_bytes(hr.at[pl.ds(0, NX - 1), pl.ds(0, NX - 1)], send.at[10])
     wait_bytes(xn.at[pl.ds(0, near_blocks)], send.at[11])
     wait_bytes(rtn.at[pl.ds(0, near_blocks)], send.at[12])
     wait_bytes(npr.at[pl.ds(0, NX - 1)], send.at[13])
@@ -501,14 +527,13 @@
     G = len(groups_of(list(range(NZ))))
     vm = pltpu.VMEM
     scratch = [
-        vm((NX, seqs, quarter), BF16),
         *[vm((NE, RB, NX * HD), BF16)] * 4,
         *[vm((NX, QB * seqs, HD), BF16)] * 2,
         pltpu.SMEM(lengths.shape, jnp.int32), pltpu.SMEM(stay_bias.shape, F32),
         vm((seqs, width), BF16), vm((1, width), F32), vm((1, width), F32),
         vm(routes.shape, jnp.int32), vm(route_weight.shape, F32),
-        vm(key_cache.shape, BF16), vm(value_cache.shape, BF16),
-        vm(out_weight.shape, BF16), vm((width, hidden), BF16), vm((width, hidden), BF16),
+        vm(key_cache.shape, BF16), vm((seqs, HD, cache_len), BF16), vm(value_cache.shape, BF16),
+        vm(out_weight.shape, BF16), vm((width, 2 * hidden), BF16),
         vm((hidden, width), BF16),
         vm((seqs, width), BF16),
         vm((NZ, seqs, kblock), BF16),
@@ -516,7 +541,7 @@
         vm((NZ, seqs, 2 * HD), BF16), vm((NZ, seqs, 2 * HD), BF16),
         vm((NZ, seqs, 2 * HD), BF16), vm((NZ, seqs, 2 * HD), BF16),
         vm((2 * seqs, cache_len), BF16),
-        vm((NX, seqs, quarter), BF16), vm((NX, seqs, quarter), BF16),
+        vm((NX, seqs, quarter), BF16), vm((NX, NX, seqs, quarter), BF16),
         vm((NE, RB, HD), BF16), vm((NX, NE, RB, HD), BF16),
         vm((NX, NE * CAP, quarter), BF16), vm((NX, NE * CAP, quarter), BF16),
         vm((NE, RB, HD), BF16), vm((NE, RB, HD), BF16),

time: 50.9 us -> 49.2 us (0.967)
  Pallas kernels: 50.2 us -> 48.5 us
    pallas_call x1, Pallas kernels: 49.6 us -> 47.9 us  [body(): pl.pallas_call(functools.partial(layer_kernel, sizes), out_shape=[pltpu.V...]
where the time goes in v4:
time: 49.2 us; the launch traced here: 49.1 us
  Pallas kernels  48.5 us (99%)
  between operations  0.65 us (1%)
    pallas_call x1, Pallas kernels, body(): pl.pallas_call(functools.partial(layer_kernel, sizes), out_shape=[pltpu.V...  47.9 us

profile of v4, /device:TPU:1, one launch (start us, length us, event | category | flops | bytes accessed | tf_op | source)
XLA Modules:
  0.0 49.1 jit_solution(9924249079703345564)
XLA Ops:
  0.6 47.9 %shard_map.175 = (bf16[16,512]{1,0:T(8,128)(2,1)S(1)}, bf16[16,128]{1,0:T(8,128)(2,1)S(1)}, bf16[16,128]{1,0:T(8,128)(2,1)S(1)}) custom-call(bf16[16,2048]{1,0:T(8,128)(2,1)} %tokens.1, bf16[16,1024,128]{2,1,0:T(8,128)(2,1)} %key_cache.1, bf16[16,1024,128]{2,1,0:T(8,128)(2,1)} %value_cache.1, s32[16]{0:T(128)} %lengths_in.1, f32[1,2048]{1,0:T(1,128)} %bitcast.4, ...), custom_call_target="tpu_custom_call" | custom-call | tf_op jit(solution)/shard_map/pallas_call | solution.py:557
  48.5 0.6 %shard_map.176 = (bf16[16,512]{1,0:T(8,128)(2,1)}, bf16[16,128]{1,0:T(8,128)(2,1)}, bf16[16,128]{1,0:T(8,128)(2,1)}) custom-call(bf16[16,512]{1,0:T(8,128)(2,1)S(1)} %get-tuple-element.6.layer_in, bf16[16,128]{1,0:T(8,128)(2,1)S(1)} %get-tuple-element.7.keys_in, bf16[16,128]{1,0:T(8,128)(2,1)S(1)} %get-tuple-element.8.values_in), custom_call_target="tpu_custom_call" | custom-call | tf_op jit(solution)/shard_map/pallas_call | solution.py:572

commit v5 on v4

--- a/solution.py
+++ b/solution.py
@@ -40,7 +40,7 @@
     tokens, key_cache, value_cache, lengths_in, attn_gain, query_weight, key_weight, value_weight,
     bias_in, out_weight, ffn_gain, gate_weight, up_weight, down_weight, routes, route_weight,
     layer_out, new_keys, new_values,
-    sbn, xn, rbn, rtn, nps, npr, lengths, stay_bias, tok, gain_a, gain_f, route_v, rweight_v, kc, kt, vc, ow, guw, dw,
+    place, sbn, xn, rbn, rtn, nps, npr, lengths, stay_bias, tok, gain_a, gain_f, route_v, rweight_v, kc, kt, vc, ow, guw, dw,
     normed, slices, wq, wkv, part_q, part_kv, got_q, got_kv,
     sticks, hp, hr, sb, xg, epart, egot, rb, rt,
     loc, kv_sem, exp_sem, send, recv, chunk_recv, group_recv, group_got,
@@ -130,10 +130,6 @@
         ).start()
     for i in range(1, NP):
         remote(wq.at[yc], wq.at[yc], send.at[1], recv.at[1], pplus(i)[1]).start()
-    ld_wk.wait()
-    ld_wv.wait()
-    for i in range(1, NP):
-        remote(wkv.at[yc], wkv.at[yc], send.at[2], recv.at[2], pplus(i)[1]).start()
     slices[pl.ds(z, 1)] = normed[:, pl.ds(pl.multiple_of(z * kblock, kblock), kblock)][None]
 
     rt[...] = jnp.zeros_like(rt)
@@ -157,6 +153,11 @@
         zt = zplus(d)
         remote(part_q.at[zt], got_q.at[z], send.at[3], recv.at[3], {"ep_0": zt}).start()
     got_q[pl.ds(z, 1)] = part_q[pl.ds(z, 1)]
+
+    ld_wk.wait()
+    ld_wv.wait()
+    for i in range(1, NP):
+        remote(wkv.at[yc], wkv.at[yc], send.at[2], recv.at[2], pplus(i)[1]).start()
 
     rows, cols = QB * seqs, NE * RB
     ld_rt.wait()
@@ -181,7 +182,7 @@
     chosen = (row // seqs == lax.rem(col, QB)) & (
         before == (lax.rem(col, RB) // QB).astype(F32)
     )
-    place = jnp.where(chosen, hit, 0.0).astype(BF16)
+    place[...] = jnp.where(chosen, hit, 0.0).T.astype(BF16)
     weighted = jnp.where(chosen, weighted, 0.0)
     weight_hi = weighted.astype(BF16)
     weight_lo = (weighted - weight_hi.astype(F32)).astype(BF16)
@@ -206,7 +207,9 @@
 
     zs = total * (HD ** -0.5) + bias_col
     live = iota((2 * seqs, cache_len), 1) < length_col
-    log_stay = jnp.where(live, -(jnp.maximum(zs, 0.0) + jnp.log1p(jnp.exp(-jnp.abs(zs)))), 0.0)
+    rest = jnp.log1p(jnp.exp(-jnp.abs(zs)))
+    log_stay = jnp.where(live, -(jnp.maximum(zs, 0.0) + rest), 0.0)
+    log_break = jnp.minimum(zs, 0.0) - rest
     blk = min(256, cache_len)
     nblk = cache_len // blk
     n = 2 * seqs
@@ -221,14 +224,14 @@
         lo = (terms - hi.astype(F32)).astype(BF16)
         return dot(hi, matrix) + dot(lo, matrix)
 
-    tri = (iota((blk, blk), 0) >= iota((blk, blk), 1)).astype(F32).astype(BF16)
-    from_here = summed_by(tri, parts)
-    from_later = summed_by(jnp.ones((blk, blk), BF16), after[:-1]) if nblk > 1 else None
+    tri = (iota((blk, blk), 0) > iota((blk, blk), 1)).astype(F32).astype(BF16)
+    in_block = summed_by(tri, parts)
+    in_later = summed_by(jnp.ones((blk, blk), BF16), after[:-1]) if nblk > 1 else None
     for b in range(nblk):
         at = slice(b * blk, (b + 1) * blk)
-        power = zs[:, at] + from_here[b * n : (b + 1) * n]
+        power = log_break[:, at] + in_block[b * n : (b + 1) * n]
         if b < nblk - 1:
-            power = power + from_later[b * n : (b + 1) * n]
+            power = power + in_later[b * n : (b + 1) * n]
         sticks[:, at] = jnp.where(live[:, at], jnp.exp(power), 0.0).astype(BF16)
 
     weights = sticks[...]
@@ -275,7 +278,7 @@
     residual = (own_tok + jnp.sum(hr[:, pl.ds(x, 1)].astype(F32), axis=(0, 1))).astype(BF16)
 
     stacked = jnp.concatenate([residual[:, q * HD : (q + 1) * HD] for q in range(QB)], axis=0)
-    outgoing = dot(place, stacked, ((0,), (0,)))
+    outgoing = dot(place[...], stacked)
     sb[...] = outgoing.reshape(NE, RB, HD).astype(BF16)
 
     for k in far_ks:
@@ -301,7 +304,7 @@
         ],
         axis=0,
     )
-    sbn[...] = dot(place, stacked, ((0,), (0,))).reshape(NE, RB, NX * HD).astype(BF16)
+    sbn[...] = dot(place[...], stacked).reshape(NE, RB, NX * HD).astype(BF16)
 
     for k in direct[::-1]:
         zt = zplus(NZ - k)
@@ -474,14 +477,27 @@
     new_keys[...] = kv[:, :HD]
     new_values[...] = kv[:, HD:]
 
+    far_blocks = len(far_ks) * NP
+    near_blocks = len(direct) * NP - 1
+
+    wait_bytes(npr.at[pl.ds(0, NX - 1)], recv.at[13])
+    near_sum = jnp.sum(npr[...].astype(F32), axis=0)
+
+    wait_bytes(rt.at[pl.ds(0, far_blocks)], recv.at[9])
+
+    back = rt[...].astype(F32).reshape(NE * RB, HD).astype(BF16)
+    routed = near_sum + dot(weight_hi, back) + dot(weight_lo, back)
+    res_f = residual.astype(F32)
+    for q in range(QB):
+        at = slice(q * HD, (q + 1) * HD)
+        layer_out[:, at] = (res_f[:, at] + routed[q * seqs : (q + 1) * seqs]).astype(BF16)
+
     wait_bytes(slices.at[pl.ds(0, NZ - 1)], send.at[0])
     wait_bytes(wq.at[pl.ds(0, NP - 1)], send.at[1])
     wait_bytes(wkv.at[pl.ds(0, NP - 1)], send.at[2])
     wait_bytes(got_q.at[pl.ds(0, NZ - 1)], send.at[3])
     wait_bytes(got_kv.at[pl.ds(0, NZ - 1)], send.at[4])
     wait_bytes(hr.at[0, pl.ds(0, NX - 1)], send.at[5])
-    far_blocks = len(far_ks) * NP
-    near_blocks = len(direct) * NP - 1
     wait_bytes(xg.at[0, pl.ds(0, far_blocks)], send.at[6])
     wait_bytes(xg.at[pl.ds(0, NX - 1), pl.ds(0, far_blocks)], send.at[7])
     wait_bytes(egot.at[pl.ds(0, NX - 1), pl.ds(0, far_blocks * CAP)], send.at[8])
@@ -489,19 +505,6 @@
     wait_bytes(xn.at[pl.ds(0, near_blocks)], send.at[11])
     wait_bytes(rtn.at[pl.ds(0, near_blocks)], send.at[12])
     wait_bytes(npr.at[pl.ds(0, NX - 1)], send.at[13])
-
-    wait_bytes(npr.at[pl.ds(0, NX - 1)], recv.at[13])
-    near_sum = jnp.sum(npr[...].astype(F32), axis=0)
-
-    wait_bytes(rt.at[pl.ds(0, far_blocks)], recv.at[9])
-
-    back = rt[...].astype(F32).reshape(NE * RB, HD).astype(BF16)
-    routed = near_sum + dot(weight_hi, back) + dot(weight_lo, back)
-    res_f = residual.astype(F32)
-    for q in range(QB):
-        at = slice(q * HD, (q + 1) * HD)
-        layer_out[:, at] = (res_f[:, at] + routed[q * seqs : (q + 1) * seqs]).astype(BF16)
-
     wait_bytes(rt.at[pl.ds(0, far_blocks)], send.at[9])
 
 def tail_kernel(layer_in, keys_in, values_in, layer_out, new_keys, new_values):
@@ -527,6 +530,7 @@
     G = len(groups_of(list(range(NZ))))
     vm = pltpu.VMEM
     scratch = [
+        vm((NE * RB, QB * seqs), BF16),
         *[vm((NE, RB, NX * HD), BF16)] * 4,
         *[vm((NX, QB * seqs, HD), BF16)] * 2,
         pltpu.SMEM(lengths.shape, jnp.int32), pltpu.SMEM(stay_bias.shape, F32),

time: 49.2 us -> 49.3 us (level)
  no operation moved by 1% of the time
where the time goes in v5:
time: 49.3 us; the launch traced here: 49.2 us
  Pallas kernels  48.5 us (98%)
  between operations  0.65 us (1%)
    pallas_call x1, Pallas kernels, body(): pl.pallas_call(functools.partial(layer_kernel, sizes), out_shape=[pltpu.V...  47.9 us

profile of v5, /device:TPU:1, one launch (start us, length us, event | category | flops | bytes accessed | tf_op | source)
XLA Modules:
  0.0 49.2 jit_solution(8983988055895565193)
XLA Ops:
  0.6 47.9 %shard_map.175 = (bf16[16,512]{1,0:T(8,128)(2,1)S(1)}, bf16[16,128]{1,0:T(8,128)(2,1)S(1)}, bf16[16,128]{1,0:T(8,128)(2,1)S(1)}) custom-call(bf16[16,2048]{1,0:T(8,128)(2,1)} %tokens.1, bf16[16,1024,128]{2,1,0:T(8,128)(2,1)} %key_cache.1, bf16[16,1024,128]{2,1,0:T(8,128)(2,1)} %value_cache.1, s32[16]{0:T(128)} %lengths_in.1, f32[1,2048]{1,0:T(1,128)} %bitcast.4, ...), custom_call_target="tpu_custom_call" | custom-call | tf_op jit(solution)/shard_map/pallas_call | solution.py:561
  48.6 0.6 %shard_map.176 = (bf16[16,512]{1,0:T(8,128)(2,1)}, bf16[16,128]{1,0:T(8,128)(2,1)}, bf16[16,128]{1,0:T(8,128)(2,1)}) custom-call(bf16[16,512]{1,0:T(8,128)(2,1)S(1)} %get-tuple-element.6.layer_in, bf16[16,128]{1,0:T(8,128)(2,1)S(1)} %get-tuple-element.7.keys_in, bf16[16,128]{1,0:T(8,128)(2,1)S(1)} %get-tuple-element.8.values_in), custom_call_target="tpu_custom_call" | custom-call | tf_op jit(solution)/shard_map/pallas_call | solution.py:576
